TPU v7x, 512 devices: a whole 4x8x8 slice. The times are simulated.
512 devices in a mesh: ep: 32 (over z, x), tp: 16 (over y, core).
Axes of the slice: x: 4, y: 8, z: 8, core: 2. Of those that a mesh axis runs over, the one named last changes fastest.
Arguments:
- mix_query: bfloat16 [8192, 2048], P('ep', 'tp'), may hold values from -6 to 6
- forget_input: bfloat16 [8192, 2048], P('ep', 'tp'), may hold values from -6 to 6
- mix_value: bfloat16 [8192, 2048], P('ep', 'tp'), may hold values from -6 to 6
- out_gate_input: bfloat16 [8192, 2048], P('ep', 'tp'), may hold values from -6 to 6
- decay_shift: float32 [8192, 16], P('ep', 'tp'), may hold values from -1.5 to 0
- forget_floor: float32 [2048], P('tp'), may hold values from 0.9 to 1
- head_gain: float32 [128], replicated, may hold values from 0.1 to 1.9
- w_mix_out: bfloat16 [2048, 2048], P(None, 'tp'), may hold values from -0.125 to 0.125
- moe_input: bfloat16 [8192, 2048], P('ep'), may hold values from -6 to 6
- moe_gain: float32 [2048], replicated, may hold values from 0.1 to 1.9
- routes: int32 [8192, 2], P('ep'), may hold values from 0 to 31, all different within a row; in each aligned block of 256 rows (0 to 255, 256 to 511, ...) at most 20 rows name the same one
- route_weight: float32 [8192, 2], P('ep'), may hold values from 0.1 to 1
- w_exp_gate: bfloat16 [32, 2048, 4096], P('ep', None, 'tp'), may hold values from -0.125 to 0.125
- w_exp_up: bfloat16 [32, 2048, 4096], P('ep', None, 'tp'), may hold values from -0.125 to 0.125
- w_exp_down: bfloat16 [32, 4096, 2048], P('ep', 'tp'), may hold values from -0.125 to 0.125
Outputs:
- mixed: bfloat16 [8192, 2048], P('ep', 'tp')
- moe_out: bfloat16 [8192, 2048], P('ep', 'tp')
Inputs may be any that keep to these rules, and one draw needn't show every extreme that they name: `routes`: at most 20 of the rows of one index of ep name one expert, and in every draw some device's rows name one expert exactly 20 times; the experts of a row differ.
All inputs are finite; a program needn't handle non-finite values.
Results may differ from a plain program's by a relative error of at most 0.02.
Values may be sent and summed in bfloat16 or wider, within the bound.
A program may use at most 64 MiB of HBM per device.

v0:
```python
import jax
import jax.numpy as jnp
from jax import lax
from jax.sharding import Mesh
from jax.sharding import PartitionSpec as P

TOP_K = 2
EP = ("ep_0", "ep_1")
TP = ("tp_0", "tp_1")


eps = 1e-06
highest_precision = lax.Precision.HIGHEST


def nothing_yet(shard, identity):
    return jax.tree.map(
        lambda a, e: jnp.broadcast_to(jnp.asarray(e, a.dtype), a.shape), shard, identity
    )


def gathered_once(shard, axis):
    leaves = jax.tree.leaves(shard)
    sequence = sorted(range(len(leaves)), key=lambda k: -leaves[k].size)
    width = (1, *leaves[sequence[0]].shape)[-1]
    lines = [
        jnp.pad(leaves[k].reshape(-1), (0, -leaves[k].size % width)).reshape(-1, width)
        for k in sequence
    ]
    both, at, found = (lax.all_gather(jnp.concatenate(lines), axis), 0, {})
    for k, line in zip(sequence, lines):
        slab = both[:, at : at + len(line)].reshape(len(both), -1)
        found[k] = slab[:, : leaves[k].size].reshape(-1, *leaves[k].shape)
        at += len(line)
    numbers = iter(range(len(leaves)))
    return jax.tree.map(lambda _: found[next(numbers)], shard)


def carried_in(shard, axes, combine, identity):
    before = start = nothing_yet(shard, identity)
    running = shard
    for axis in reversed(axes):
        peers, index = (lax.axis_size(axis), lax.axis_index(axis))
        pieces = gathered_once(
            jax.tree.map(
                lambda part, kind: part.astype(kind), running, (jnp.bfloat16, jnp.bfloat16)
            ),
            axis,
        )
        inside, running = (start, start)
        for k in range(peers):
            passed = k < index
            running = combine(
                running, jax.tree.map(lambda part, own: part[k].astype(own.dtype), pieces, shard)
            )
            inside = jax.tree.map(lambda new, old: jnp.where(passed, new, old), running, inside)
        before = combine(inside, before)
    return before


def sent_to_all(shard, axis):
    peers = lax.axis_size(axis)
    return lax.all_to_all(
        jnp.broadcast_to(shard[None], (peers, *shard.shape)), axis, 0, 0, tiled=True
    )


def laid_out(tiles, dim):
    tiles = jnp.moveaxis(tiles, 0, dim)
    lengths = tiles.shape
    return tiles.reshape(*lengths[:dim], lengths[dim] * lengths[dim + 1], *lengths[dim + 2 :])


def gather_directly(shard, axis, dim):
    tiles = sent_to_all(shard, axis)
    return laid_out(tiles, dim)


def split_up(shard, dim, peers):
    lengths = shard.shape
    tiles = shard.reshape(*lengths[:dim], peers, lengths[dim] // peers, *lengths[dim + 1 :])
    return jnp.moveaxis(tiles, dim, 0)


def scatter_pairs(shard, chips, core, dim):
    sizes = (lax.axis_size(chips), lax.axis_size(core))
    tiles = split_up(shard, dim, sizes[0] * sizes[1])
    inside = tiles.shape[1:]
    tiles = tiles.reshape(*sizes, *inside).swapaxes(0, 1).reshape(-1, *inside)
    tiles = lax.psum_scatter(tiles, core, scatter_dimension=0, tiled=True)
    return lax.psum_scatter(tiles, chips, scatter_dimension=0, tiled=True)[0]


def chain_step(earlier, later):
    return (earlier[0] * later[0], later[0][:, :, None] * earlier[1] + later[1])


def token_mixer(
    mix_query,
    forget_input,
    mix_value,
    out_gate_input,
    decay_shift,
    forget_floor,
    head_gain,
    w_mix_out,
):
    length = mix_query.shape[0]
    heads_here = decay_shift.shape[1]
    head_size = head_gain.shape[0]
    gate_input = forget_input.astype(jnp.float32)
    forget = forget_floor + (1.0 - forget_floor) * jax.nn.sigmoid(gate_input)
    input_gate = (1.0 - forget_floor) * jax.nn.sigmoid(-gate_input)
    log_decay = jnp.log(forget) + jnp.repeat(decay_shift, head_size, axis=1)

    def by_head(array):
        return array.reshape(length, heads_here, head_size).transpose(1, 0, 2)

    running_decay = jnp.cumsum(by_head(log_decay), axis=1)
    query_rows = by_head(mix_query.astype(jnp.float32)) * jnp.exp(running_decay)
    head_keys = by_head(input_gate)
    values = by_head(mix_value.astype(jnp.float32))
    scores = jnp.einsum(
        "htk,hsk->hts", query_rows, head_keys * jnp.exp(-running_decay), precision=highest_precision
    )
    causal = jnp.arange(length)[:, None] >= jnp.arange(length)[None, :]
    scores = jnp.where(causal[None, :, :], scores, 0.0)
    within_block_output = jnp.einsum("hts,hsv->htv", scores, values, precision=highest_precision)
    closing_total = running_decay[:, -1, :]
    carried_over_state = jnp.einsum(
        "gbx,gbi->gxi",
        head_keys * jnp.exp(closing_total[:, None, :] - running_decay),
        values,
        precision=highest_precision,
    )
    incoming_state = carried_in(
        (jnp.exp(closing_total), carried_over_state),
        EP,
        chain_step,
        (jnp.ones_like(closing_total), jnp.zeros_like(carried_over_state)),
    )[1]
    block_result = within_block_output + jnp.einsum(
        "rsd,rda->rsa", query_rows, incoming_state, precision=highest_precision
    )
    inverse = lax.rsqrt(jnp.mean(block_result * block_result, axis=2, keepdims=True) + eps)
    gated = by_head(jax.nn.silu(out_gate_input.astype(jnp.float32)))
    normed_heads = (block_result * inverse * head_gain * gated).transpose(1, 0, 2)
    head_out = normed_heads.reshape(length, heads_here * head_size).astype(jnp.bfloat16)
    mixed = jnp.dot(
        lax.all_gather(head_out, TP, axis=1, tiled=True),
        w_mix_out,
        preferred_element_type=jnp.float32,
    )
    return mixed.astype(jnp.bfloat16)


def experts_layer(moe_input, moe_gain, routes, route_weight, w_exp_gate, w_exp_up, w_exp_down):
    row_count = moe_input.shape[0]
    expert_count = lax.axis_size(EP)
    capacity = 5 * row_count * TOP_K // (4 * expert_count)
    token_rows = moe_input.astype(jnp.float32)
    inverse = lax.rsqrt(jnp.mean(token_rows * token_rows, axis=1, keepdims=True) + eps)
    normed = (token_rows * inverse * moe_gain).astype(jnp.bfloat16)
    flat_ids = routes.reshape(-1)
    pair_count = flat_ids.shape[0]
    one_hot = (flat_ids[:, None] == jnp.arange(expert_count, dtype=jnp.int32)[None, :]).astype(
        jnp.int32
    )
    earlier_count = jnp.cumsum(one_hot, axis=0) - one_hot
    ranks = jnp.sum(earlier_count * one_hot, axis=1)
    slot_ids = flat_ids * capacity + ranks
    owners = (
        jnp.zeros((expert_count * capacity,), jnp.int32)
        .at[slot_ids]
        .set(jnp.arange(pair_count, dtype=jnp.int32) // TOP_K)
    )
    filled = (
        jnp.zeros((expert_count * capacity,), jnp.bfloat16)
        .at[slot_ids]
        .set(jnp.ones((pair_count,), jnp.bfloat16))
    )
    outgoing = normed[owners] * filled[:, None]
    w_gate = w_exp_gate[0]
    w_up = w_exp_up[0]
    w_down = w_exp_down[0]
    width = normed.shape[1] // lax.axis_size(TP)
    own_slice = lax.dynamic_slice_in_dim(outgoing, lax.axis_index(TP) * width, width, 1)
    arrived = lax.all_to_all(own_slice, EP, split_axis=0, concat_axis=0, tiled=True)
    portion = gather_directly(arrived, TP, 1)
    gate_sum = jnp.dot(portion, w_gate, preferred_element_type=jnp.float32)
    up_sum = jnp.dot(portion, w_up, preferred_element_type=jnp.float32)
    hidden = (jax.nn.silu(gate_sum) * up_sum).astype(jnp.bfloat16)
    partial_value = jnp.dot(hidden, w_down, preferred_element_type=jnp.float32)
    summed = (
        scatter_pairs(partial_value.astype(jnp.bfloat16), "tp_0", "tp_1", 1)
        .astype(jnp.float32)
        .astype(jnp.bfloat16)
    )
    returned = lax.all_to_all(summed, EP, split_axis=0, concat_axis=0, tiled=True)
    picked = returned[slot_ids].astype(jnp.float32).reshape(row_count, TOP_K, returned.shape[1])
    combined = jnp.sum(picked * route_weight[:, :, None], axis=1)
    return combined.astype(jnp.bfloat16)


def body(
    mix_query,
    forget_input,
    mix_value,
    out_gate_input,
    decay_shift,
    forget_floor,
    head_gain,
    w_mix_out,
    moe_input,
    moe_gain,
    routes,
    route_weight,
    w_exp_gate,
    w_exp_up,
    w_exp_down,
):
    mixed = token_mixer(
        mix_query,
        forget_input,
        mix_value,
        out_gate_input,
        decay_shift,
        forget_floor,
        head_gain,
        w_mix_out,
    )
    moe_out = experts_layer(
        moe_input, moe_gain, routes, route_weight, w_exp_gate, w_exp_up, w_exp_down
    )
    return (mixed, moe_out)


def solution(mesh):
    torus = Mesh(mesh.devices.reshape(8, 4, 8, 2), ("ep_0", "ep_1", "tp_0", "tp_1"))
    placed = (
        P(EP, TP),
        P(EP, TP),
        P(EP, TP),
        P(EP, TP),
        P(EP, TP),
        P(TP),
        P(),
        P(None, TP),
        P(EP, None),
        P(),
        P(EP, None),
        P(EP, None),
        P(EP, None, TP),
        P(EP, None, TP),
        P(EP, TP, None),
    )
    return jax.shard_map(
        body, mesh=torus, in_specs=placed, out_specs=(P(EP, TP), P(EP, TP)), check_vma=False
    )
```

profile of v0, /device:TPU:1, one launch (start us, length us, event | category | flops | bytes accessed | tf_op | source)
XLA Modules:
  0.0 226.4 jit_solution(9882331451542621476)
XLA Ops:
  8.1 0.9 copy.57
  9.0 0.1 eq.29
  9.2 0.1 eq.25
  9.3 0.7 broadcast_multiply_fusion
  10.0 1.2 reduce-window.16
  11.2 0.2 slice_reduce_fusion
  11.5 0.1 copy.56
  11.6 0.1 mul.373
  11.9 2.4 %scatter_custom_fusion = s32[640]{0:T(1024)S(1)} fusion(s32[512]{0:T(512)S(1)} %bitcast.177, s32[512]{0:T(512)S(1)} %add_select_fusion, s32[]{:T(128)} %constant.34.clone.1), kind=kCustom, calls=%fused_computation.173 | custom fusion | bytes 2564 | tf_op jit(solution)/shard_map/scatter | solution.py:175
  14.3 1.5 fusion
  15.9 1.0 fusion.2
  16.9 4.1 %gather_fusion = bf16[640,2048]{1,0:T(8,128)(2,1)} fusion(bf16[256,2048]{1,0:T(8,128)(2,1)S(1)} %fusion.2, s32[1024]{0:T(1024)S(1)} %pad_clamp_fusion.1), kind=kCustom, calls=%fused_computation | custom fusion | bytes 5245440 | tf_op jit(solution)/shard_map/gather | solution.py:182
  21.0 3.8 %scatter_custom_fusion.1 = bf16[640]{0:T(1024)(128)(2,1)S(1)} fusion(s32[512]{0:T(512)S(1)} %bitcast.178, bf16[512]{0:T(512)(128)(2,1)S(1)} %broadcast.266, bf16[]{:T(256)} %constant.85.clone.1), kind=kCustom, calls=%fused_computation.177 | custom fusion | bytes 1282 | tf_op jit(solution)/shard_map/scatter | solution.py:180
  24.7 1.1 dynamic-slice_multiply_fusion
  25.9 23.5 %all_to_all.26 = bf16[32,20,128]{2,1,0:T(8,128)(2,1)S(1)} all-to-all(bf16[32,20,128]{2,1,0:T(8,128)(2,1)S(1)} %all_to_all.17), channel_id=1, replica_groups=mesh['ep_0'=8,'ep_1'=4,'tp_0'=8,'tp_1'=2] {'ep_0','ep_1'}, dimensions={0} | all-to-all | bytes 327680 | tf_op jit(solution)/shard_map/all_to_all | solution.py:188
  49.4 0.2 copy.60
  49.6 0.3 broadcast_in_dim.28
  49.9 71.8 %all_to_all.27 = bf16[16,640,128]{1,2,0:T(8,128)(2,1)S(1)} all-to-all(bf16[16,640,128]{1,2,0:T(8,128)(2,1)S(1)} %broadcast_in_dim.28), channel_id=1, replica_groups=mesh['ep_0'=8,'ep_1'=4,'tp_0'=8,'tp_1'=2] {'tp_0','tp_1'}, dimensions={0} | all-to-all | bytes 5242880 | tf_op jit(solution)/shard_map/all_to_all | solution.py:63
  121.7 1.5 copy-done.2
  123.2 0.9 fusion.7
  124.1 0.3 copy-done.13
  124.4 6.1 %fusion.3 = bf16[80,16,8,128]{3,2,1,0:T(8,128)(2,1)} fusion(bf16[1,256,2048]{2,1,0:T(8,128)(2,1)S(1)} %copy-done, bf16[640,2048]{0,1:T(8,128)(2,1)} %bitcast.175, bf16[1,2048,256]{2,1,0:T(8,128)(2,1)S(1)} %copy-done.13, f32[640,256]{1,0:T(8,128)S(1)} %fusion.7), kind=kOutput, calls=%fused_computation.11 | convolution fusion | flops 1344471040 | bytes 7995392 | tf_op jit(solution)/shard_map/dot_general | solution.py:193
  130.5 2.4 %copy.68 = bf16[80,16,8,128]{3,2,0,1:T(8,128)(2,1)S(1)} copy(bf16[80,16,8,128]{3,2,1,0:T(8,128)(2,1)} %fusion.3) | data formatting | bytes 5242880 | tf_op jit(solution)/shard_map/reshape | solution.py:81
  132.9 1.7 copy.62
  134.8 0.7 copy-done.5
  135.8 0.1 copy.52
  135.9 0.1 fusion.156
  136.1 0.1 copy.53
  136.3 0.1 copy.54
  136.4 0.2 broadcast.258
  136.8 0.2 slice_reduce_fusion.1
  137.0 0.2 fusion.93
  137.2 0.3 convolution_convert_fusion.2
  137.5 9.5 %all-gather.2 = bf16[4,129,128]{2,1,0:T(8,128)(2,1)S(1)} all-gather(bf16[1,129,128]{2,1,0:T(8,128)(2,1)S(1)} %maximum_bitcast_fusion), channel_id=2, replica_groups=mesh['ep_0'=8,'ep_1'=4,'tp_0'=8,'tp_1'=2] {'ep_1'}, dimensions={0}, use_global_device_ids=true | all-gather | bytes 165120 | tf_op jit(solution)/shard_map/all_gather | solution.py:30
  147.4 0.1 fusion.94
  147.6 19.3 %all-gather.3 = bf16[8,129,128]{2,1,0:T(8,128)(2,1)S(1)} all-gather(bf16[1,129,128]{2,1,0:T(8,128)(2,1)S(1)} %maximum_bitcast_fusion.1), channel_id=3, replica_groups=mesh['ep_0'=8,'ep_1'=4,'tp_0'=8,'tp_1'=2] {'ep_0'}, dimensions={0}, use_global_device_ids=true | all-gather | bytes 297216 | tf_op jit(solution)/shard_map/all_gather | solution.py:30
  166.8 0.4 convolution_select_fusion
  167.3 0.3 fusion.157
  167.6 0.6 multiply_reduce_fusion
  168.2 0.7 fusion.42
  169.0 17.1 %reduce-scatter.5.cloned.1.call-done = bf16[1,640,128]{2,1,0:T(8,128)(2,1)} async-done(((bf16[8,640,128]{2,1,0:T(8,128)(2,1)}), bf16[1,640,128]{2,1,0:T(8,128)(2,1)}) %reduce-scatter.5.cloned.1.call-update) | async-done | bytes 163856 | tf_op jit(solution)/shard_map/reduce_scatter | solution.py:91
  186.1 1.6 all_to_all.20
  187.7 9.9 %all-to-all-start.2 = ((bf16[32,20,128]{2,1,0:T(8,128)(2,1)}), bf16[32,20,128]{2,1,0:T(8,128)(2,1)S(1)}, u32[]{:S(2)}, u32[]{:S(2)}) async-start(bf16[32,20,128]{2,1,0:T(8,128)(2,1)} %all_to_all.20), calls=%async_computation.4 | async-start | bytes 393216 | tf_op jit(solution)/shard_map/all_to_all | solution.py:199
  197.6 0.1 copy.63
  197.8 16.4 %all-gather.6.cloned.1.call-done = bf16[256,2048]{0,1:T(8,128)(2,1)} async-done(((bf16[256,128]{0,1:T(8,128)(2,1)}), bf16[256,2048]{0,1:T(8,128)(2,1)}) %all-gather.6.cloned.1.call-update) | async-done | bytes 1048592 | tf_op jit(solution)/shard_map/all_gather | solution.py:150
  214.1 2.3 %convolution_convert_fusion.1 = bf16[256,128]{1,0:T(8,128)(2,1)} fusion(bf16[256,2048]{0,1:T(8,128)(2,1)} %all-gather.6.cloned.1.call-done, bf16[2048,128]{1,0:T(8,128)(2,1)S(1)} %copy-done.3), kind=kOutput, calls=%fused_computation.16 | convolution fusion | flops 134250496 | bytes 1638400 | tf_op jit(solution)/shard_map/dot_general | solution.py:149
  216.5 1.3 gather_fusion.1
  217.9 1.1 fusion.12
  (67 shorter events, 1.4 us)
Async XLA Ops:
  8.0 116.1 %copy-start = (bf16[1,256,2048]{2,1,0:T(8,128)(2,1)S(1)}, bf16[1,256,2048]{2,1,0:T(8,128)(2,1)}, u32[]{:S(2)}) copy-start(bf16[1,256,2048]{2,1,0:T(8,128)(2,1)} %param.29) | copy-start | bytes 3145732
  8.0 7.9 %copy-start.1 = (bf16[256,2048]{1,0:T(8,128)(2,1)S(1)}, bf16[256,2048]{1,0:T(8,128)(2,1)}, u32[]{:S(2)}) copy-start(bf16[256,2048]{1,0:T(8,128)(2,1)} %param.23) | copy-start | bytes 3145732
  8.0 139.0 %reduce-scatter.3.cloned.1.call-start = ((), (), s32[]{:S(2)}) async-start(), calls=%async_computation.6 | async-start | bytes 3932160 | tf_op jit(solution)/shard_map/reduce_scatter | solution.py:90
  49.9 73.3 %copy-start.12 = (bf16[1,2048,256]{2,1,0:T(8,128)(2,1)S(1)}, bf16[1,2048,256]{2,1,0:T(8,128)(2,1)}, u32[]{:S(2)}) copy-start(bf16[1,2048,256]{2,1,0:T(8,128)(2,1)} %param.27) | copy-start | bytes 3145732
  121.7 1.5 copy-start.2
  123.2 1.2 copy-start.13
  134.6 0.8 copy-start.5
  134.6 1.0 copy-start.10
  134.6 1.0 copy-start.9
  134.7 2.6 %copy-start.4 = (bf16[256,128]{1,0:T(8,128)(2,1)S(1)}, bf16[256,128]{1,0:T(8,128)(2,1)}, u32[]{:S(2)}) copy-start(bf16[256,128]{1,0:T(8,128)(2,1)} %param.17) | copy-start | bytes 196612
  134.7 12.4 %copy-start.6 = (bf16[256,128]{1,0:T(8,128)(2,1)S(1)}, bf16[256,128]{1,0:T(8,128)(2,1)}, u32[]{:S(2)}) copy-start(bf16[256,128]{1,0:T(8,128)(2,1)} %param.15) | copy-start | bytes 196612
  134.7 12.6 %copy-start.7 = (bf16[256,128]{1,0:T(8,128)(2,1)S(1)}, bf16[256,128]{1,0:T(8,128)(2,1)}, u32[]{:S(2)}) copy-start(bf16[256,128]{1,0:T(8,128)(2,1)} %param.18) | copy-start | bytes 196612
  134.7 51.4 %reduce-scatter.5.cloned.1.call-start = ((), (), s32[]{:S(2)}) async-start(), calls=%async_computation.7 | async-start | bytes 1474560 | tf_op jit(solution)/shard_map/reduce_scatter | solution.py:91
  137.5 30.8 %copy-start.11 = (f32[128]{0:T(128)S(1)}, f32[128]{0:T(128)}, u32[]{:S(2)}) copy-start(f32[128]{0:T(128)} %param.21) | copy-start | bytes 1540
  147.0 50.6 %copy-start.8 = (f32[256,2]{0,1:T(2,128)S(1)}, f32[256,2]{0,1:T(2,128)}, u32[]{:S(2)}) copy-start(f32[256,2]{0,1:T(2,128)} %param.26) | copy-start | bytes 6148
  147.0 67.1 %copy-start.3 = (bf16[2048,128]{1,0:T(8,128)(2,1)S(1)}, bf16[2048,128]{1,0:T(8,128)(2,1)}, u32[]{:S(2)}) copy-start(bf16[2048,128]{1,0:T(8,128)(2,1)} %param.22) | copy-start | bytes 1572868
  147.0 67.1 %all-gather.6.cloned.1.call-start = ((), (), s32[]{:S(2)}) async-start(), calls=%async_computation.5 | async-start | bytes 1114112 | tf_op jit(solution)/shard_map/all_gather | solution.py:150
  187.7 28.8 %all-to-all-start.2 = ((bf16[32,20,128]{2,1,0:T(8,128)(2,1)}), bf16[32,20,128]{2,1,0:T(8,128)(2,1)S(1)}, u32[]{:S(2)}, u32[]{:S(2)}) async-start(bf16[32,20,128]{2,1,0:T(8,128)(2,1)} %all_to_all.20), calls=%async_computation.4 | async-start | bytes 393216 | tf_op jit(solution)/shard_map/all_to_all | solution.py:199
Sparse Core Ops, SparseCore 0:
  134.8 9.7 reduce-scatter.2
  147.4 38.5 reduce-scatter.4
Sparse Core Ops, SparseCore 1:
  169.1 45.0 all-gather.5
where the time goes:
time: 227 us; the launch traced here: 226 us
  blocking collectives  124 us (55%)
  waiting for transfers between devices  33.5 us (15%)
  local copies, waits for them, and re-layouts  23.8 us (10%)
  between operations  16 us (7%)
  matrix products  11 us (5%)
  starting transfers between devices  10 us (4%)
  other arithmetic  8.08 us (4%)
    all_to_all x1, blocking collectives, sent_to_all(): lax.all_to_all(jnp.broadcast_to(shard[None], (peers, *shard.shape)), axis...  71.8 us
    all_gather x2, blocking collectives, gathered_once(): both, at, found = (lax.all_gather(jnp.concatenate(lines), axis), 0, {})  28.7 us
    all_to_all x1, blocking collectives, experts_layer(): lax.all_to_all(own_slice, EP, split_axis=0, concat_axis=0, tiled=True)  23.5 us
    reduce_scatter x1, waiting for transfers between devices, scatter_pairs(): return lax.psum_scatter(tiles, chips, scatter_dimension=0, tiled=True)[0]  17.1 us
    all_gather x1, waiting for transfers between devices, token_mixer(): lax.all_gather(head_out, TP, axis=1, tiled=True)  16.4 us
    all_to_all x1, starting transfers between devices, experts_layer(): lax.all_to_all(summed, EP, split_axis=0, concat_axis=0, tiled=True)  9.92 us
    dot_general x1, matrix products, experts_layer(): partial_value = jnp.dot(hidden, w_down, preferred_element_type=jnp.float32)  6.11 us
  transfers between devices with their start and end apart: 4, of which 2 were waited for; matrix products, arithmetic and copies ran while one was open for 3% of the time, Pallas kernels for 0%

commit v1 on v0

v1 whole, which is shorter than its diff:
```python
import jax
import jax.numpy as jnp
from jax import lax
from jax.experimental import pallas as pl
from jax.experimental.pallas import tpu as pltpu
from jax.sharding import Mesh
from jax.sharding import PartitionSpec as P

EP = ("ep_0", "ep_1")
TP = ("tp_0", "tp_1")
NZ, NX, NY = 8, 4, 8
N_EP = NZ * NX
ROWS = 256
CAP = 20
D = 2048
DK = 128
FPD = 256
HALF = CAP * N_EP // 2
SLOTS = CAP * N_EP
DBLK = 48
RBLK = 32
SUB = 64
PACK = DK + 16
EPS = 1e-6
MESH = pl.DeviceIdType.MESH
F32 = jnp.float32
BF16 = jnp.bfloat16
I32 = jnp.int32
HIGH = lax.Precision.HIGHEST

SEND_ORDER = (8, 7, 9, 6, 10, 5, 11, 4, 12, 3, 13, 2, 14, 1, 15, 0)
RETURN_ORDER = sorted(range(1, N_EP), key=lambda o: -min(o, N_EP - o))
CHUNK_ORDER = (4, 3, 5, 2, 6, 1, 7, 0)


def ones_where(mask):
    return jnp.where(mask, 1.0, 0.0).astype(BF16)


def nt_dot(a, b, precision=None):
    return lax.dot_general(
        a, b, (((1,), (1,)), ((), ())), precision=precision, preferred_element_type=F32
    )


def mm(a, b, precision=None):
    return jnp.dot(a, b, precision=precision, preferred_element_type=F32)


def iota(shape, dim):
    return lax.broadcasted_iota(I32, shape, dim)


def kernel(
    q_ref, f_ref, v_ref, og_ref, shift_ref, floor_ref, hgain_ref, wmix_hbm,
    moe_hbm, gain_ref, routes_ref, rw_ref, wg_hbm, wu_hbm, wd_hbm,
    mixed_ref, moe_ref,
    moe_v, mine_v, wg_v, wu_v, wd_v, wmix_v, norm_v,
    sbuf, rbuf, xs, accg, accu, hid, part, pout, pin, rsend, rrecv,
    rout, rin, qh_v, ql_v, sx, sz, qd_v, hs,
    lsem, wsem, dsend, drecv, asend, arecv, psend, precv, csend, crecv,
    ssend, srecv, bsend, brecv, xsend, xrecv, zsend, zrecv, hsend, hrecv,
    gsend, grecv,
):
    z = lax.axis_index("ep_0")
    x = lax.axis_index("ep_1")
    y = lax.axis_index("tp_0")
    c = lax.axis_index("tp_1")
    me = z * NX + x

    def at_ep(e):
        return (lax.div(e, NX), lax.rem(e, NX), y, c)

    up = (z, x, lax.rem(y + 1, NY), c)
    down = (z, x, lax.rem(y + NY - 1, NY), c)
    partner = (z, x, y, 1 - c)

    def remote(src, dst, send, recv, device):
        return pltpu.make_async_remote_copy(
            src_ref=src, dst_ref=dst, send_sem=send, recv_sem=recv,
            device_id=device, device_id_type=MESH,
        )

    pending = []

    def push(src, dst, send, recv, device):
        copy = remote(src, dst, send, recv, device)
        copy.start()
        pending.append(copy)

    def await_in(dst, send, recv):
        remote(dst, dst, send, recv, partner).wait_recv()

    rows_in = []
    for i in range(4):
        rows_in.append(pltpu.make_async_copy(
            moe_hbm.at[pl.ds(64 * i, 64), :], moe_v.at[pl.ds(64 * i, 64), :], lsem.at[i]))
    rows_in.append(pltpu.make_async_copy(
        moe_hbm.at[:, pl.ds(pl.multiple_of(y * FPD, FPD), FPD)], mine_v, lsem.at[4]))
    for copy in rows_in:
        copy.start()

    barrier = pltpu.get_barrier_semaphore()

    def greet(o, carry):
        pl.semaphore_signal(
            barrier, inc=1, device_id=at_ep(lax.rem(me + o, N_EP)), device_id_type=MESH)
        return carry

    lax.fori_loop(1, N_EP, greet, 0)
    for device in (up, down, partner):
        pl.semaphore_signal(barrier, inc=1, device_id=device, device_id_type=MESH)

    weights_in = [
        pltpu.make_async_copy(wg_hbm, wg_v, wsem.at[0]),
        pltpu.make_async_copy(wu_hbm, wu_v, wsem.at[1]),
        pltpu.make_async_copy(wmix_hbm, wmix_v, wsem.at[2]),
    ]
    for i in range(NY):
        for h in range(2):
            column = pl.multiple_of(i * FPD + lax.rem(c + h, 2) * DK, DK)
            weights_in.append(pltpu.make_async_copy(
                wd_hbm.at[:, pl.ds(column, DK)],
                wd_v.at[i, :, pl.ds(h * DK, DK)], wsem.at[3 + 2 * i + h]))
    for copy in weights_in:
        copy.start()

    e0, e1 = routes_ref[0:1, :], routes_ref[1:2, :]
    ids = iota((N_EP, ROWS), 0)
    one0, one1 = ids == e0, ids == e1
    ones = jnp.concatenate([ones_where(one0), ones_where(one1)], axis=0)
    strict = ones_where(iota((ROWS, ROWS), 0) < iota((ROWS, ROWS), 1))
    earlier = mm(ones, strict)
    total0 = jnp.sum(jnp.where(one0, 1.0, 0.0), axis=1, keepdims=True)
    rank0 = jnp.sum(jnp.where(one0, earlier[:N_EP], 0.0), axis=0, keepdims=True).astype(I32)
    rank1 = jnp.sum(
        jnp.where(one1, earlier[N_EP:] + total0, 0.0), axis=0, keepdims=True).astype(I32)

    for i in range(4):
        rows_in[i].wait()
    rows_in[4].wait()
    gain = gain_ref[pl.ds(y, 1), :]
    for i in range(4):
        block = moe_v[64 * i:64 * i + 64, :].astype(F32)
        mean = jnp.sum(block * block, axis=1, keepdims=True) * (1.0 / D)
        own = mine_v[64 * i:64 * i + 64, :].astype(F32)
        norm_v[64 * i:64 * i + 64, :] = (own * lax.rsqrt(mean + EPS) * gain).astype(BF16)

    parity = lax.rem(x + c, 2)
    target0 = jnp.where((e0 & 1) == parity, (e0 >> 1) * DBLK + rank0, -1000)
    target1 = jnp.where((e1 & 1) == parity, (e1 >> 1) * DBLK + rank1, -1000)
    n0, n1 = norm_v[:, :DK], norm_v[:, DK:]
    for g in range(4):
        spot = iota((4 * DBLK, ROWS), 0) + 4 * DBLK * g
        first = ones_where((spot == target0) | (spot == target1))
        second = ones_where((spot == target0 + CAP) | (spot == target1 + CAP))
        rows = (mm(first, n0) + mm(second, n1)).astype(BF16)
        sbuf[4 * g:4 * g + 4] = rows.reshape(4, DBLK, DK)

    pl.semaphore_wait(barrier, N_EP + 2)

    def dispatch(o):
        expert = lax.rem(me + 2 * o + c, N_EP)
        return remote(sbuf.at[lax.div(expert, 2)], rbuf.at[lax.div(me, 2)],
                      dsend.at[o], drecv.at[o], at_ep(expert))

    own_copy = pltpu.make_async_copy(
        sbuf.at[lax.div(me, 2)], rbuf.at[lax.div(me, 2)], lsem.at[5])
    for o in SEND_ORDER:
        if o:
            dispatch(o).start()
        else:
            @pl.when(c == 1)
            def _():
                dispatch(0).start()

            @pl.when(c == 0)
            def _():
                own_copy.start()

    floor = floor_ref[...]
    pre = f_ref[...].astype(F32)
    forget = floor + (1.0 - floor) * jax.nn.sigmoid(pre)
    keys = (1.0 - floor) * jax.nn.sigmoid(-pre)
    shift = jnp.transpose(jnp.broadcast_to(shift_ref[...], (DK, ROWS)))
    log_decay = jnp.log(forget) + shift
    lower = jnp.where(iota((ROWS, ROWS), 0) >= iota((ROWS, ROWS), 1), 1.0, 0.0)
    running = mm(lower, log_decay, HIGH)
    values = v_ref[...].astype(F32)
    query = q_ref[...].astype(F32)
    closing = running[ROWS - 1:ROWS, :]
    values_t = jnp.transpose(values)
    state_t = mm(values_t, keys * jnp.exp(closing - running), HIGH)
    sx[x, 0:DK, :] = state_t.astype(BF16)
    sx[x, DK:PACK, :] = jnp.broadcast_to(jnp.exp(closing), (PACK - DK, DK)).astype(BF16)
    for dx in range(1, NX):
        push(sx.at[x], sx.at[x], xsend.at[dx], xrecv.at[dx],
             (z, lax.rem(x + dx, NX), y, c))

    causal = iota((SUB, SUB), 0) >= iota((SUB, SUB), 1)
    local = []
    for i in range(ROWS // SUB):
        lo, hi = i * SUB, (i + 1) * SUB
        decay_i, query_i = running[lo:hi], query[lo:hi]
        middle = running[lo + SUB // 2 - 1:lo + SUB // 2]
        scores = jnp.where(causal, nt_dot(
            query_i * jnp.exp(decay_i - middle), keys[lo:hi] * jnp.exp(middle - decay_i),
            HIGH), 0.0)
        out = mm(scores, values[lo:hi], HIGH)
        if i:
            start = running[lo - 1:lo]
            scores = nt_dot(query_i * jnp.exp(decay_i - start),
                            keys[:lo] * jnp.exp(start - running[:lo]), HIGH)
            out = out + mm(scores, values[:lo], HIGH)
        local.append(out)
    qd_v[0] = jnp.concatenate(local, axis=0)
    qd_v[1] = query * jnp.exp(running)

    slot0 = (e0 * RBLK + rank0).astype(F32)
    slot1 = (e1 * RBLK + rank1).astype(F32)
    which = iota((DK, ROWS), 0)
    table = jnp.where(which == 0, slot0, jnp.where(which == 1, slot1, jnp.where(
        which == 2, rw_ref[0:1, :], jnp.where(which == 3, rw_ref[1:2, :], 0.0))))
    table = jnp.transpose(table)
    place0, place1 = table[:, 0:1].astype(I32), table[:, 1:2].astype(I32)
    for g in range(4):
        spot = iota((ROWS, 256), 1) + 256 * g
        weight = jnp.where(spot == place0, table[:, 2:3], 0.0) + jnp.where(
            spot == place1, table[:, 3:4], 0.0)
        high = weight.astype(BF16)
        qh_v[:, 256 * g:256 * g + 256] = high
        ql_v[:, 256 * g:256 * g + 256] = (weight - high.astype(F32)).astype(BF16)

    for o in SEND_ORDER:
        source = lax.rem(me + N_EP - 2 * o + N_EP - c, N_EP)
        if o:
            await_in(rbuf.at[lax.div(source, 2)], dsend.at[o], drecv.at[o])
        else:
            @pl.when(c == 1)
            def _():
                await_in(rbuf.at[lax.div(source, 2)], dsend.at[0], drecv.at[0])

            @pl.when(c == 0)
            def _():
                own_copy.wait()
    row, col = iota((4 * CAP, 4 * DBLK), 0), iota((4 * CAP, 4 * DBLK), 1)
    spot = row + (DBLK - CAP) * ((row * 3277) >> 16)
    packs = [ones_where(col == spot + CAP * h) for h in range(2)]
    for g in range(4):
        block = rbuf[4 * g:4 * g + 4].reshape(4 * DBLK, DK)
        for h in range(2):
            xs[y, c, g // 2, (g % 2) * 80:(g % 2) * 80 + 80, h * DK:(h + 1) * DK] = mm(
                packs[h], block).astype(BF16)

    def slab(j):
        return lax.rem(y + j, NY)

    def ring_send(buf, direction, hop, sub, send, recv):
        j = (NY - hop) % NY if direction == 0 else hop
        index = direction * 8 + hop * 2 + sub
        push(buf.at[slab(j), c, sub], buf.at[slab(j), c, sub], send.at[index], recv.at[index],
             up if direction == 0 else down)

    def ring_take(buf, direction, hop, sub, send, recv):
        j = (NY - hop) % NY if direction == 0 else hop
        index = direction * 8 + (hop - 1) * 2 + sub
        await_in(buf.at[slab(j), c, sub], send.at[index], recv.at[index])
        return j

    def pair_send(buf, j, sub, send, recv):
        push(buf.at[slab(j), c, sub], buf.at[slab(j), c, sub],
             send.at[2 * j + sub], recv.at[2 * j + sub], partner)

    def pair_take(buf, j, sub, send, recv):
        await_in(buf.at[slab(j), 1 - c, sub], send.at[2 * j + sub], recv.at[2 * j + sub])

    far, near = ((0, 0), (1, 1)), ((0, 1), (1, 0))

    def gather_start(buf, send, recv, psend, precv):
        for direction, sub in far + near:
            ring_send(buf, direction, 0, sub, send, recv)
        for sub in range(2):
            pair_send(buf, 0, sub, psend, precv)

    def gather_hop(buf, hop, send, recv, psend, precv):
        for direction, sub in far + (near if hop < 4 else ()):
            j = ring_take(buf, direction, hop, sub, send, recv)
            if hop < (4 if (direction, sub) in far else 3):
                ring_send(buf, direction, hop, sub, send, recv)
            pair_send(buf, j, sub, psend, precv)

    gather_start(xs, asend, arecv, psend, precv)

    def read_state(ref, k):
        return ref[k, DK:PACK, :].astype(F32)[0:1], ref[k, 0:DK, :].astype(F32)

    def step(before, after):
        return before[0] * after[0], after[0] * before[1] + after[1]

    def prefix(ref, count, index):
        running = (jnp.ones((1, DK), F32), jnp.zeros((DK, DK), F32))
        inside = running
        for k in range(count):
            running = step(running, read_state(ref, k))
            inside = tuple(jnp.where(k < index, a, b) for a, b in zip(running, inside))
        return inside, running

    for dx in range(1, NX):
        await_in(sx.at[lax.rem(x + NX - dx, NX)], xsend.at[dx], xrecv.at[dx])
    inside_x, whole = prefix(sx, NX, x)
    sz[z, 0:DK, :] = whole[1].astype(BF16)
    sz[z, DK:PACK, :] = jnp.broadcast_to(whole[0], (PACK - DK, DK)).astype(BF16)
    for dz in (4, 3, 5, 2, 6, 1, 7):
        push(sz.at[z], sz.at[z], zsend.at[dz], zrecv.at[dz],
             (lax.rem(z + dz, NZ), x, y, c))

    weights_in[0].wait()
    weights_in[1].wait()

    def expert_in(j, first=False):
        for sub in range(2):
            pair_take(xs, j, sub, psend, precv)
        rows = xs[slab(j)].reshape(SLOTS, FPD)
        depth = pl.ds(pl.multiple_of(slab(j) * FPD, FPD), FPD)
        if first:
            accg[...] = mm(rows, wg_v[depth, :])
            accu[...] = mm(rows, wu_v[depth, :])
        else:
            accg[...] += mm(rows, wg_v[depth, :])
            accu[...] += mm(rows, wu_v[depth, :])

    gather_hop(xs, 1, asend, arecv, psend, precv)
    expert_in(0, True)
    gather_hop(xs, 2, asend, arecv, psend, precv)
    expert_in(1)
    expert_in(7)

    for dz in range(1, NZ):
        await_in(sz.at[lax.rem(z + NZ - dz, NZ)], zsend.at[dz], zrecv.at[dz])
    before, _ = prefix(sz, NZ, z)
    incoming = step(before, inside_x)[1]
    result = qd_v[0] + nt_dot(qd_v[1], incoming, HIGH)
    inverse = lax.rsqrt(jnp.mean(result * result, axis=1, keepdims=True) + EPS)
    head_out = result * inverse * hgain_ref[...] * jax.nn.silu(og_ref[...].astype(F32))
    hs[y, c] = head_out.astype(BF16).reshape(2, ROWS // 2, DK)

    gather_hop(xs, 3, asend, arecv, psend, precv)
    expert_in(2)
    expert_in(6)
    gather_hop(xs, 4, asend, arecv, psend, precv)
    expert_in(3)
    expert_in(5)
    expert_in(4)

    for i in range(4):
        block = slice(160 * i, 160 * i + 160)
        hid[block, :] = (jax.nn.silu(accg[block, :]) * accu[block, :]).astype(BF16)
    for copy in weights_in[3:]:
        copy.wait()

    def expert_out(j):
        partial = mm(hid[...], wd_v[slab(j)]).astype(BF16)
        part[j] = partial[:, :DK]
        pout[j] = partial[:, DK:]
        push(pout.at[j], pin.at[j], csend.at[j], crecv.at[j], partner)

    def chip_sum(j, sub):
        block = slice(HALF * sub, HALF * sub + HALF)
        return part[j, block, :].astype(F32) + pin[j, block, :].astype(F32)

    def sum_send(direction, step, sub, value):
        index = direction * 8 + step * 2 + sub
        rsend[direction, step, sub] = value.astype(BF16)
        push(rsend.at[direction, step, sub], rrecv.at[direction, step, sub],
             ssend.at[index], srecv.at[index], up if direction == 0 else down)

    def sum_take(direction, step, sub):
        index = direction * 8 + step * 2 + sub
        await_in(rrecv.at[direction, step, sub], ssend.at[index], srecv.at[index])
        return rrecv[direction, step, sub].astype(F32)

    def ready(j):
        await_in(pin.at[j], csend.at[j], crecv.at[j])

    def target(direction, sub, step):
        j = (4 if (direction, sub) in far else 3) - step
        return j % NY if direction == 0 else -j % NY

    for j in (4, 3, 5):
        expert_out(j)
    ready(4)
    for direction, sub in far:
        sum_send(direction, 0, sub, chip_sum(target(direction, sub, 0), sub))
    ready(3)
    ready(5)
    for direction, sub in near:
        sum_send(direction, 0, sub, chip_sum(target(direction, sub, 0), sub))
    for j in (2, 6, 1, 7, 0):
        expert_out(j)
    last = {}
    for step_at in range(1, 5):
        if step_at == 1:
            late = (2, 6)
        elif step_at == 2:
            late = (1, 7)
        elif step_at == 3:
            late = (0,)
        else:
            late = ()
        for direction, sub in far:
            if step_at < 4:
                value = sum_take(direction, step_at - 1, sub)
                sum_send(direction, step_at, sub,
                         value + chip_sum(target(direction, sub, step_at), sub))
        for j in late:
            ready(j)
        for direction, sub in near:
            if step_at < 3:
                value = sum_take(direction, step_at - 1, sub)
                sum_send(direction, step_at, sub,
                         value + chip_sum(target(direction, sub, step_at), sub))
    for direction, sub in near:
        last[sub] = chip_sum(0, sub) + sum_take(direction, 2, sub)
    for direction, sub in far:
        last[sub] = last[sub] + sum_take(direction, 3, sub)

    row, col = iota((4 * RBLK, 4 * CAP), 0), iota((4 * RBLK, 4 * CAP), 1)
    spread = ones_where((col == (row >> 5) * CAP + (row & 31)) & ((row & 31) < CAP))
    for g in range(8):
        value = last[g // 4][(g % 4) * 80:(g % 4) * 80 + 80].astype(BF16)
        rout[4 * g:4 * g + 4] = mm(spread, value).astype(BF16).reshape(4, RBLK, DK)
    for o in RETURN_ORDER:
        there = lax.rem(me + o, N_EP)
        push(rout.at[lax.rem(there + x, 2) * 16 + lax.div(there, 2)], rin.at[me],
             bsend.at[o], brecv.at[o], at_ep(there))
    rin[me] = rout[lax.div(me, 2)]

    gather_start(hs, hsend, hrecv, gsend, grecv)
    weights_in[2].wait()

    def project(j):
        for sub in range(2):
            pair_take(hs, j, sub, gsend, grecv)
        heads = hs[slab(j)].reshape(2, ROWS, DK)
        rows = jnp.concatenate([heads[0], heads[1]], axis=1)
        return mm(rows, wmix_v[pl.ds(pl.multiple_of(slab(j) * FPD, FPD), FPD), :])

    gather_hop(hs, 1, hsend, hrecv, gsend, grecv)
    mixed = project(0)
    gather_hop(hs, 2, hsend, hrecv, gsend, grecv)
    mixed += project(1) + project(7)
    gather_hop(hs, 3, hsend, hrecv, gsend, grecv)
    mixed += project(2) + project(6)
    gather_hop(hs, 4, hsend, hrecv, gsend, grecv)
    mixed += project(3) + project(5)
    mixed += project(4)
    mixed_ref[...] = mixed.astype(BF16)

    for o in RETURN_ORDER:
        await_in(rin.at[lax.rem(me + N_EP - o, N_EP)], bsend.at[o], brecv.at[o])
    returned = rin[...].reshape(N_EP * RBLK, DK)
    moe_ref[...] = (mm(qh_v[...], returned) + mm(ql_v[...], returned)).astype(BF16)

    for copy in pending:
        copy.wait_send()
    for o in SEND_ORDER:
        if o:
            dispatch(o).wait_send()
        else:
            @pl.when(c == 1)
            def _():
                dispatch(0).wait_send()


def body(
    mix_query, forget_input, mix_value, out_gate_input, decay_shift, forget_floor, head_gain,
    w_mix_out, moe_input, moe_gain, routes, route_weight, w_exp_gate, w_exp_up, w_exp_down,
):
    vmem = pl.BlockSpec(memory_space=pltpu.VMEM)
    hbm = pl.BlockSpec(memory_space=pl.ANY)
    sem = pltpu.SemaphoreType.DMA
    outs = jax.ShapeDtypeStruct((ROWS, DK), BF16)
    return pl.pallas_call(
        kernel,
        out_shape=(outs, outs),
        in_specs=[vmem] * 7 + [hbm] * 2 + [vmem] * 3 + [hbm] * 3,
        out_specs=(vmem, vmem),
        scratch_shapes=[
            pltpu.VMEM((ROWS, D), BF16),
            pltpu.VMEM((ROWS, FPD), BF16),
            pltpu.VMEM((D, FPD), BF16),
            pltpu.VMEM((D, FPD), BF16),
            pltpu.VMEM((NY, FPD, FPD), BF16),
            pltpu.VMEM((D, DK), BF16),
            pltpu.VMEM((ROWS, FPD), BF16),
            pltpu.VMEM((16, DBLK, DK), BF16),
            pltpu.VMEM((16, DBLK, DK), BF16),
            pltpu.VMEM((NY, 2, 2, HALF // 2, FPD), BF16),
            pltpu.VMEM((SLOTS, FPD), F32),
            pltpu.VMEM((SLOTS, FPD), F32),
            pltpu.VMEM((SLOTS, FPD), BF16),
            pltpu.VMEM((NY, SLOTS, DK), BF16),
            pltpu.VMEM((NY, SLOTS, DK), BF16),
            pltpu.VMEM((NY, SLOTS, DK), BF16),
            pltpu.VMEM((2, 4, 2, HALF, DK), BF16),
            pltpu.VMEM((2, 4, 2, HALF, DK), BF16),
            pltpu.VMEM((N_EP, RBLK, DK), BF16),
            pltpu.VMEM((N_EP, RBLK, DK), BF16),
            pltpu.VMEM((ROWS, N_EP * RBLK), BF16),
            pltpu.VMEM((ROWS, N_EP * RBLK), BF16),
            pltpu.VMEM((NX, PACK, DK), BF16),
            pltpu.VMEM((NZ, PACK, DK), BF16),
            pltpu.VMEM((2, ROWS, DK), F32),
            pltpu.VMEM((NY, 2, 2, ROWS // 2, DK), BF16),
            sem((6,)), sem((19,)), sem((16,)), sem((16,)), sem((16,)), sem((16,)),
            sem((16,)), sem((16,)), sem((8,)), sem((8,)), sem((16,)), sem((16,)),
            sem((N_EP,)), sem((N_EP,)), sem((NX,)), sem((NX,)), sem((NZ,)), sem((NZ,)),
            sem((16,)), sem((16,)), sem((16,)), sem((16,)),
        ],
        compiler_params=pltpu.CompilerParams(collective_id=0, has_side_effects=True),
        name="step",
    )(
        mix_query, forget_input, mix_value, out_gate_input,
        decay_shift.reshape(1, ROWS), forget_floor.reshape(1, DK), head_gain.reshape(1, DK),
        w_mix_out, moe_input, moe_gain.reshape(NY, FPD), routes.T, route_weight.T,
        w_exp_gate[0], w_exp_up[0], w_exp_down[0],
    )


def solution(mesh):
    torus = Mesh(mesh.devices.reshape(NZ, NX, NY, 2), ("ep_0", "ep_1", "tp_0", "tp_1"))
    placed = (
        P(EP, TP), P(EP, TP), P(EP, TP), P(EP, TP), P(EP, TP), P(TP), P(), P(None, TP),
        P(EP, None), P(), P(EP, None), P(EP, None), P(EP, None, TP), P(EP, None, TP),
        P(EP, TP, None),
    )
    return jax.shard_map(
        body, mesh=torus, in_specs=placed, out_specs=(P(EP, TP), P(EP, TP)), check_vma=False
    )
```

time: 227 us -> 84.2 us (0.37)
  blocking collectives: 124 us -> 0 us
  Pallas kernels: 0 us -> 79.9 us
  waiting for transfers between devices: 33.5 us -> 0 us
  local copies, waits for them, and re-layouts: 23.8 us -> 3.43 us
  between operations: 16 us -> 0.66 us
  matrix products: 11 us -> 0 us
  starting transfers between devices: 10 us -> 0 us
  other arithmetic: 8.08 us -> 0 us
    all_to_all x2 -> x0, blocking collectives: 95.3 us -> none  [the longest x1 71.8 us: sent_to_all(): lax.all_to_all(jnp.broadcast_to(shard[None], (peers, *shard.shape)), axis...]
    pallas_call x0 -> x1, Pallas kernels: none -> 79.9 us  [body(): pl.pallas_call(kernel, out_shape=(outs, outs), in_specs=[vmem] * 7 + [hbm...]
    all_gather x2 -> x0, blocking collectives: 28.7 us -> none  [gathered_once(): both, at, found = (lax.all_gather(jnp.concatenate(lines), axis), 0, {})]
    reduce_scatter x2 -> x0, waiting for transfers between devices: 17.1 us -> none  [the longest x1 17.1 us: scatter_pairs(): return lax.psum_scatter(tiles, chips, scatter_dimension=0, tiled=True)[0]]
    all_gather x1 -> x0, waiting for transfers between devices: 16.4 us -> none  [token_mixer(): lax.all_gather(head_out, TP, axis=1, tiled=True)]
    dot_general x7 -> x0, matrix products: 11 us -> none  [the longest x1 6.11 us: experts_layer(): partial_value = jnp.dot(hidden, w_down, preferred_element_type=jnp.float32)]
    all_to_all x1 -> x0, starting transfers between devices: 9.92 us -> none  [experts_layer(): lax.all_to_all(summed, EP, split_axis=0, concat_axis=0, tiled=True)]
    scatter x2 -> x0, local copies, waits for them, and re-layouts: 6.21 us -> none  [the longest x1 3.77 us: experts_layer(): filled = jnp.zeros((expert_count * capacity,), jnp.bfloat16).at[slot_ids]...]
  transfers between devices with their start and end apart: 4 -> 0, of which waited for: 2 -> 0; matrix products, arithmetic and copies ran while one was open for 3% -> 0% of each run, Pallas kernels for 0% -> 0%
where the time goes in v1:
time: 84.2 us; the launch traced here: 84 us
  Pallas kernels  79.9 us (95%)
  local copies, waits for them, and re-layouts  3.43 us (4%)
    pallas_call x1, Pallas kernels, body(): pl.pallas_call(kernel, out_shape=(outs, outs), in_specs=[vmem] * 7 + [hbm...  79.9 us
    unnamed x6, local copies, waits for them, and re-layouts  2.83 us

profile of v1, /device:TPU:1, one launch (start us, length us, event | category | flops | bytes accessed | tf_op | source)
XLA Modules:
  0.0 84.0 jit_solution(1132971842792082136)
XLA Ops:
  0.6 0.0 copy-start.1
  0.6 0.7 copy-done.1
  1.3 0.6 reshape.19.gain_ref
  1.9 79.9 %step.1 = (bf16[256,128]{1,0:T(8,128)(2,1)}, bf16[256,128]{1,0:T(8,128)(2,1)}) custom-call(bf16[256,128]{1,0:T(8,128)(2,1)} %q_ref.1, bf16[256,128]{1,0:T(8,128)(2,1)} %f_ref.1, bf16[256,128]{1,0:T(8,128)(2,1)} %v_ref.1, bf16[256,128]{1,0:T(8,128)(2,1)} %og_ref.1, f32[1,256]{1,0:T(1,128)} %bitcast.13, f32[1,128]{1,0:T(1,128)} %bitcast.14, ...), custom_call_target="tpu_custom_call" | custom-call | tf_op jit(solution)/shard_map/step/pallas_call | solution.py:483
  81.8 0.0 copy-start
  81.8 1.5 %copy.19 = bf16[256,128]{1,0:T(8,128)(2,1)} copy(bf16[256,128]{1,0:T(8,128)(2,1)} %get-tuple-element.4) | data formatting | bytes 131072
  83.3 0.0 copy-done
  83.3 0.6 copy.20
Async XLA Ops:
  0.6 0.7 copy-start.1
  81.8 1.5 %copy-start = (bf16[256,128]{1,0:T(8,128)(2,1)S(1)}, bf16[256,128]{1,0:T(8,128)(2,1)}, u32[]{:S(2)}) copy-start(bf16[256,128]{1,0:T(8,128)(2,1)} %get-tuple-element.5) | copy-start | bytes 196612

commit v2 on v1

v2 whole, which is shorter than its diff:
```python
import jax
import jax.numpy as jnp
from jax import lax
from jax.experimental import pallas as pl
from jax.experimental.pallas import tpu as pltpu
from jax.sharding import Mesh
from jax.sharding import PartitionSpec as P

EP = ("ep_0", "ep_1")
TP = ("tp_0", "tp_1")
NZ, NX, NY = 8, 4, 8
N_EP = NZ * NX
ROWS = 256
CAP = 20
D = 2048
DK = 128
FPD = 256
HALF = CAP * N_EP // 2
SLOTS = CAP * N_EP
DBLK = 40
RBLK = 24
SUB = 64
PACK = DK + 16
EPS = 1e-6
MESH = pl.DeviceIdType.MESH
F32 = jnp.float32
BF16 = jnp.bfloat16
I32 = jnp.int32
HIGH = lax.Precision.HIGHEST

SEND_ORDER = (8, 7, 9, 6, 10, 5, 11, 4, 12, 3, 13, 2, 14, 1, 15, 0)
RETURN_ORDER = sorted(range(1, N_EP), key=lambda o: -min(o, N_EP - o))
CHUNK_ORDER = (4, 3, 5, 2, 6, 1, 7, 0)


def ones_where(mask):
    return jnp.where(mask, 1.0, 0.0).astype(BF16)


def nt_dot(a, b, precision=None):
    return lax.dot_general(
        a, b, (((1,), (1,)), ((), ())), precision=precision, preferred_element_type=F32
    )


def mm(a, b, precision=None):
    return jnp.dot(a, b, precision=precision, preferred_element_type=F32)


def iota(shape, dim):
    return lax.broadcasted_iota(I32, shape, dim)


def kernel(
    q_hbm, f_hbm, v_hbm, og_hbm, shift_ref, floor_ref, hgain_ref, wmix_hbm,
    moe_hbm, gain_ref, routes_ref, rw_ref, wg_hbm, wu_hbm, wd_hbm,
    mixed_ref, moe_ref,
    mixer_v, moe_v, mine_v, wg_v, wu_v, wd_v, wmix_v, norm_v,
    sbuf, rbuf, xs, accg, accu, hid, part, pout, pin, rsend, rrecv,
    rout, rin, qh_v, ql_v, sx, sz, qd_v, hs,
    lsem, wsem, dsend, drecv, asend, arecv, psend, precv, csend, crecv,
    ssend, srecv, bsend, brecv, xsend, xrecv, zsend, zrecv, hsend, hrecv,
    gsend, grecv,
):
    z = lax.axis_index("ep_0")
    x = lax.axis_index("ep_1")
    y = lax.axis_index("tp_0")
    c = lax.axis_index("tp_1")
    me = z * NX + x

    def at_ep(e):
        return (lax.div(e, NX), lax.rem(e, NX), y, c)

    up = (z, x, lax.rem(y + 1, NY), c)
    down = (z, x, lax.rem(y + NY - 1, NY), c)
    partner = (z, x, y, 1 - c)

    def remote(src, dst, send, recv, device):
        return pltpu.make_async_remote_copy(
            src_ref=src, dst_ref=dst, send_sem=send, recv_sem=recv,
            device_id=device, device_id_type=MESH,
        )

    pending = []

    def push(src, dst, send, recv, device):
        copy = remote(src, dst, send, recv, device)
        copy.start()
        pending.append(copy)

    def await_in(dst, send, recv):
        remote(dst, dst, send, recv, partner).wait_recv()

    rows_in = []
    for i in range(4):
        rows_in.append(pltpu.make_async_copy(
            moe_hbm.at[pl.ds(64 * i, 64), :], moe_v.at[pl.ds(64 * i, 64), :], lsem.at[i]))
    rows_in.append(pltpu.make_async_copy(
        moe_hbm.at[:, pl.ds(pl.multiple_of(y * FPD, FPD), FPD)], mine_v.at[0], lsem.at[4]))
    rows_in.append(pltpu.make_async_copy(
        moe_hbm.at[:, pl.ds(pl.multiple_of(lax.rem(y + NY // 2, NY) * FPD, FPD), FPD)],
        mine_v.at[1], lsem.at[6]))
    for copy in rows_in:
        copy.start()
    mixer_in = [
        pltpu.make_async_copy(ref, mixer_v.at[i], lsem.at[7 + i])
        for i, ref in enumerate((f_hbm, v_hbm, q_hbm, og_hbm))]
    for copy in mixer_in:
        copy.start()

    barrier = pltpu.get_barrier_semaphore()

    def greet(o, carry):
        pl.semaphore_signal(
            barrier, inc=1, device_id=at_ep(lax.rem(me + o, N_EP)), device_id_type=MESH)
        return carry

    lax.fori_loop(1, N_EP, greet, 0)
    for device in (up, down, partner):
        pl.semaphore_signal(barrier, inc=1, device_id=device, device_id_type=MESH)

    weights_in = [
        pltpu.make_async_copy(wg_hbm, wg_v, wsem.at[0]),
        pltpu.make_async_copy(wu_hbm, wu_v, wsem.at[1]),
        pltpu.make_async_copy(wmix_hbm, wmix_v, wsem.at[2]),
    ]
    for i in range(NY):
        for h in range(2):
            column = pl.multiple_of(i * FPD + lax.rem(c + h, 2) * DK, DK)
            weights_in.append(pltpu.make_async_copy(
                wd_hbm.at[:, pl.ds(column, DK)],
                wd_v.at[i, :, pl.ds(h * DK, DK)], wsem.at[3 + 2 * i + h]))
    for copy in weights_in:
        copy.start()

    e0, e1 = routes_ref[0:1, :], routes_ref[1:2, :]
    ids = iota((N_EP, ROWS), 0)
    one0, one1 = ids == e0, ids == e1
    ones = jnp.concatenate([ones_where(one0), ones_where(one1)], axis=0)
    strict = ones_where(iota((ROWS, ROWS), 0) < iota((ROWS, ROWS), 1))
    earlier = mm(ones, strict)
    total0 = jnp.sum(jnp.where(one0, 1.0, 0.0), axis=1, keepdims=True)
    rank0 = jnp.sum(jnp.where(one0, earlier[:N_EP], 0.0), axis=0, keepdims=True).astype(I32)
    rank1 = jnp.sum(
        jnp.where(one1, earlier[N_EP:] + total0, 0.0), axis=0, keepdims=True).astype(I32)

    for i in range(4):
        rows_in[i].wait()
    rows_in[4].wait()
    rows_in[5].wait()
    halves = (y, lax.rem(y + NY // 2, NY))
    gains = [gain_ref[:, pl.ds(pl.multiple_of(k * FPD, FPD), FPD)] for k in halves]
    for i in range(4):
        block = moe_v[64 * i:64 * i + 64, :].astype(F32)
        mean = jnp.sum(block * block, axis=1, keepdims=True) * (1.0 / D)
        for k in range(2):
            own = mine_v[k, 64 * i:64 * i + 64, :].astype(F32)
            norm_v[k, 64 * i:64 * i + 64, :] = (
                own * lax.rsqrt(mean + EPS) * gains[k]).astype(BF16)

    parity = lax.rem(x + c, 2)
    target0 = jnp.where((e0 & 1) == parity, (e0 >> 1) * DBLK + rank0, -1000)
    target1 = jnp.where((e1 & 1) == parity, (e1 >> 1) * DBLK + rank1, -1000)
    n0 = jnp.concatenate([norm_v[0, :, :DK], norm_v[1, :, :DK]], axis=1)
    n1 = jnp.concatenate([norm_v[0, :, DK:], norm_v[1, :, DK:]], axis=1)
    for g in range(4):
        spot = iota((4 * DBLK, ROWS), 0) + 4 * DBLK * g
        first = ones_where((spot == target0) | (spot == target1))
        second = ones_where((spot == target0 + CAP) | (spot == target1 + CAP))
        rows = (mm(first, n0) + mm(second, n1)).astype(BF16)
        for k in range(2):
            sbuf[k, 4 * g:4 * g + 4] = rows[:, k * DK:(k + 1) * DK].reshape(4, DBLK, DK)

    pl.semaphore_wait(barrier, N_EP + 2)

    def dispatch(k, o):
        expert = lax.rem(me + 2 * o + c, N_EP)
        return remote(sbuf.at[k, lax.div(expert, 2)], rbuf.at[k, lax.div(me, 2)],
                      dsend.at[16 * k + o], drecv.at[16 * k + o], at_ep(expert))

    own_copies = [pltpu.make_async_copy(
        sbuf.at[k, lax.div(me, 2)], rbuf.at[k, lax.div(me, 2)], lsem.at[k * 6 + 5])
        for k in range(2)]
    for k in range(2):
        for o in SEND_ORDER:
            if o:
                dispatch(k, o).start()
            else:
                @pl.when(c == 1)
                def _():
                    dispatch(k, 0).start()

                @pl.when(c == 0)
                def _():
                    own_copies[k].start()

    floor = floor_ref[...]
    for copy in mixer_in:
        copy.wait()
    pre = mixer_v[0].astype(F32)
    forget = floor + (1.0 - floor) * jax.nn.sigmoid(pre)
    keys = (1.0 - floor) * jax.nn.sigmoid(-pre)
    shift = jnp.transpose(jnp.broadcast_to(shift_ref[...], (DK, ROWS)))
    log_decay = jnp.log(forget) + shift
    lower = jnp.where(iota((ROWS, ROWS), 0) >= iota((ROWS, ROWS), 1), 1.0, 0.0)
    running = mm(lower, log_decay, HIGH)
    values = mixer_v[1].astype(F32)
    query = mixer_v[2].astype(F32)
    closing = running[ROWS - 1:ROWS, :]
    values_t = jnp.transpose(values)
    state_t = mm(values_t, keys * jnp.exp(closing - running), HIGH)
    sx[x, 0:DK, :] = state_t.astype(BF16)
    sx[x, DK:PACK, :] = jnp.broadcast_to(jnp.exp(closing), (PACK - DK, DK)).astype(BF16)
    for dx in range(1, NX):
        push(sx.at[x], sx.at[x], xsend.at[dx], xrecv.at[dx],
             (z, lax.rem(x + dx, NX), y, c))

    def arrived(k):
        for o in SEND_ORDER:
            source = lax.rem(me + N_EP - 2 * o + N_EP - c, N_EP)
            slot = rbuf.at[k, lax.div(source, 2)]
            if o:
                await_in(slot, dsend.at[16 * k + o], drecv.at[16 * k + o])
            else:
                @pl.when(c == 1)
                def _():
                    await_in(slot, dsend.at[16 * k], drecv.at[16 * k])

                @pl.when(c == 0)
                def _():
                    own_copies[k].wait()

    row, col = iota((4 * CAP, 4 * DBLK), 0), iota((4 * CAP, 4 * DBLK), 1)
    spot = row + (DBLK - CAP) * ((row * 3277) >> 16)
    packs = [ones_where(col == spot + CAP * h) for h in range(2)]

    def pack(k):
        arrived(k)
        for g in range(4):
            block = rbuf[k, 4 * g:4 * g + 4].reshape(4 * DBLK, DK)
            for h in range(2):
                xs[halves[k], c, g // 2, (g % 2) * 80:(g % 2) * 80 + 80,
                   h * DK:(h + 1) * DK] = mm(packs[h], block).astype(BF16)

    pack(0)

    def slab(j):
        return lax.rem(y + j, NY)

    def ring_send(buf, direction, hop, sub, send, recv):
        j = (NY - hop) % NY if direction == 0 else hop
        index = direction * 8 + hop * 2 + sub
        push(buf.at[slab(j), c, sub], buf.at[slab(j), c, sub], send.at[index], recv.at[index],
             up if direction == 0 else down)

    def ring_take(buf, direction, hop, sub, send, recv):
        j = (NY - hop) % NY if direction == 0 else hop
        index = direction * 8 + (hop - 1) * 2 + sub
        await_in(buf.at[slab(j), c, sub], send.at[index], recv.at[index])
        return j

    def pair_send(buf, j, sub, send, recv):
        push(buf.at[slab(j), c, sub], buf.at[slab(j), c, sub],
             send.at[2 * j + sub], recv.at[2 * j + sub], partner)

    def pair_take(buf, j, sub, send, recv):
        await_in(buf.at[slab(j), 1 - c, sub], send.at[2 * j + sub], recv.at[2 * j + sub])

    far, near = ((0, 0), (1, 1)), ((0, 1), (1, 0))

    def gather_start(buf, send, recv, psend, precv):
        for direction, sub in far + near:
            ring_send(buf, direction, 0, sub, send, recv)
        for sub in range(2):
            pair_send(buf, 0, sub, psend, precv)

    def gather_hop(buf, hop, send, recv, psend, precv):
        for direction, sub in far + (near if hop < 4 else ()):
            j = ring_take(buf, direction, hop, sub, send, recv)
            if hop < (4 if (direction, sub) in far else 3):
                ring_send(buf, direction, hop, sub, send, recv)
            pair_send(buf, j, sub, psend, precv)

    for sub in range(2):
        for direction in range(2):
            ring_send(xs, direction, 0, sub, asend, arecv)
        pair_send(xs, 0, sub, psend, precv)

    def rows_hop(hop, sub):
        for direction in range(2):
            j = ring_take(xs, direction, hop, sub, asend, arecv)
            if hop < 3:
                ring_send(xs, direction, hop, sub, asend, arecv)
            pair_send(xs, j, sub, psend, precv)


    def read_state(ref, k):
        return ref[k, DK:PACK, :].astype(F32)[0:1], ref[k, 0:DK, :].astype(F32)

    def step(before, after):
        return before[0] * after[0], after[0] * before[1] + after[1]

    def prefix(ref, count, index):
        running = (jnp.ones((1, DK), F32), jnp.zeros((DK, DK), F32))
        inside = running
        for k in range(count):
            running = step(running, read_state(ref, k))
            inside = tuple(jnp.where(k < index, a, b) for a, b in zip(running, inside))
        return inside, running

    for dx in range(1, NX):
        await_in(sx.at[lax.rem(x + NX - dx, NX)], xsend.at[dx], xrecv.at[dx])
    inside_x, whole = prefix(sx, NX, x)
    sz[z, 0:DK, :] = whole[1].astype(BF16)
    sz[z, DK:PACK, :] = jnp.broadcast_to(whole[0], (PACK - DK, DK)).astype(BF16)

    def along_z(dz):
        return remote(sz.at[z], sz.at[z], zsend.at[dz], zrecv.at[dz],
                      (lax.rem(z + dz, NZ), x, y, c))

    for dz in range(1, NZ):
        @pl.when(z + dz < NZ)
        def _():
            along_z(dz).start()

    causal = iota((SUB, SUB), 0) >= iota((SUB, SUB), 1)
    local = []
    for i in range(ROWS // SUB):
        lo, hi = i * SUB, (i + 1) * SUB
        decay_i, query_i = running[lo:hi], query[lo:hi]
        middle = running[lo + SUB // 2 - 1:lo + SUB // 2]
        scores = jnp.where(causal, nt_dot(
            query_i * jnp.exp(decay_i - middle), keys[lo:hi] * jnp.exp(middle - decay_i),
            HIGH), 0.0)
        out = mm(scores, values[lo:hi], HIGH)
        if i:
            start = running[lo - 1:lo]
            scores = nt_dot(query_i * jnp.exp(decay_i - start),
                            keys[:lo] * jnp.exp(start - running[:lo]), HIGH)
            out = out + mm(scores, values[:lo], HIGH)
        local.append(out)
    qd_v[0] = jnp.concatenate(local, axis=0)
    qd_v[1] = query * jnp.exp(running)


    weights_in[0].wait()
    weights_in[1].wait()

    def expert_in(j, first=False):
        for sub in range(2):
            pair_take(xs, j, sub, psend, precv)
        rows = xs[slab(j)].reshape(SLOTS, FPD)
        depth = pl.ds(pl.multiple_of(slab(j) * FPD, FPD), FPD)
        if first:
            accg[...] = mm(rows, wg_v[depth, :])
            accu[...] = mm(rows, wu_v[depth, :])
        else:
            accg[...] += mm(rows, wg_v[depth, :])
            accu[...] += mm(rows, wu_v[depth, :])

    rows_hop(1, 0)
    rows_hop(1, 1)
    expert_in(0, True)
    rows_hop(2, 0)
    expert_in(1)
    rows_hop(2, 1)
    expert_in(7)
    pack(1)
    for sub in range(2):
        pair_send(xs, 4, sub, psend, precv)

    slot0 = (e0 * RBLK + rank0).astype(F32)
    slot1 = (e1 * RBLK + rank1).astype(F32)
    which = iota((DK, ROWS), 0)
    table = jnp.where(which == 0, slot0, jnp.where(which == 1, slot1, jnp.where(
        which == 2, rw_ref[0:1, :], jnp.where(which == 3, rw_ref[1:2, :], 0.0))))
    table = jnp.transpose(table)
    place0, place1 = table[:, 0:1].astype(I32), table[:, 1:2].astype(I32)
    for g in range(N_EP * RBLK // 256):
        spot = iota((ROWS, 256), 1) + 256 * g
        weight = jnp.where(spot == place0, table[:, 2:3], 0.0) + jnp.where(
            spot == place1, table[:, 3:4], 0.0)
        high = weight.astype(BF16)
        qh_v[:, 256 * g:256 * g + 256] = high
        ql_v[:, 256 * g:256 * g + 256] = (weight - high.astype(F32)).astype(BF16)

    rows_hop(3, 0)
    expert_in(2)
    expert_in(6)
    expert_in(4)

    for dz in range(1, NZ):
        @pl.when(z >= dz)
        def _():
            await_in(sz.at[lax.rem(z + NZ - dz, NZ)], zsend.at[dz], zrecv.at[dz])

    before, _ = prefix(sz, NZ, z)
    incoming = step(before, inside_x)[1]
    result = qd_v[0] + nt_dot(qd_v[1], incoming, HIGH)
    inverse = lax.rsqrt(jnp.mean(result * result, axis=1, keepdims=True) + EPS)
    head_out = result * inverse * hgain_ref[...] * jax.nn.silu(mixer_v[3].astype(F32))
    hs[y, c] = head_out.astype(BF16).reshape(2, ROWS // 2, DK)

    gather_start(hs, hsend, hrecv, gsend, grecv)
    rows_hop(3, 1)
    expert_in(3)
    expert_in(5)

    for i in range(4):
        block = slice(160 * i, 160 * i + 160)
        hid[block, :] = (jax.nn.silu(accg[block, :]) * accu[block, :]).astype(BF16)
    for copy in weights_in[3:]:
        copy.wait()

    def expert_out(j):
        partial = mm(hid[...], wd_v[slab(j)]).astype(BF16)
        part[j] = partial[:, :DK]
        pout[j] = partial[:, DK:]
        push(pout.at[j], pin.at[j], csend.at[j], crecv.at[j], partner)

    def chip_sum(j, sub):
        block = slice(HALF * sub, HALF * sub + HALF)
        return part[j, block, :].astype(F32) + pin[j, block, :].astype(F32)

    def sum_send(direction, step, sub, value):
        index = direction * 8 + step * 2 + sub
        rsend[direction, step, sub] = value.astype(BF16)
        push(rsend.at[direction, step, sub], rrecv.at[direction, step, sub],
             ssend.at[index], srecv.at[index], up if direction == 0 else down)

    def sum_take(direction, step, sub):
        index = direction * 8 + step * 2 + sub
        await_in(rrecv.at[direction, step, sub], ssend.at[index], srecv.at[index])
        return rrecv[direction, step, sub].astype(F32)

    def ready(j):
        await_in(pin.at[j], csend.at[j], crecv.at[j])

    def target(direction, sub, step):
        j = (4 if (direction, sub) in far else 3) - step
        return j % NY if direction == 0 else -j % NY

    for j in (4, 3, 5):
        expert_out(j)
    gather_hop(hs, 1, hsend, hrecv, gsend, grecv)
    ready(4)
    for direction, sub in far:
        sum_send(direction, 0, sub, chip_sum(target(direction, sub, 0), sub))
    ready(3)
    ready(5)
    for direction, sub in near:
        sum_send(direction, 0, sub, chip_sum(target(direction, sub, 0), sub))
    for j in (2, 6):
        expert_out(j)
    gather_hop(hs, 2, hsend, hrecv, gsend, grecv)
    for j in (1, 7, 0):
        expert_out(j)
    weights_in[2].wait()

    def project(j):
        for sub in range(2):
            pair_take(hs, j, sub, gsend, grecv)
        heads = hs[slab(j)].reshape(2, ROWS, DK)
        rows = jnp.concatenate([heads[0], heads[1]], axis=1)
        return mm(rows, wmix_v[pl.ds(pl.multiple_of(slab(j) * FPD, FPD), FPD), :])

    last = {}
    for step_at in range(1, 5):
        if step_at == 1:
            late = (2, 6)
        elif step_at == 2:
            late = (1, 7)
        elif step_at == 3:
            late = (0,)
        else:
            late = ()
            mixed += project(1) + project(7) + project(2) + project(6)
        for direction, sub in far:
            if step_at < 4:
                value = sum_take(direction, step_at - 1, sub)
                sum_send(direction, step_at, sub,
                         value + chip_sum(target(direction, sub, step_at), sub))
        for j in late:
            ready(j)
        for direction, sub in near:
            if step_at < 3:
                value = sum_take(direction, step_at - 1, sub)
                sum_send(direction, step_at, sub,
                         value + chip_sum(target(direction, sub, step_at), sub))
        if step_at == 1:
            gather_hop(hs, 3, hsend, hrecv, gsend, grecv)
            mixed = project(0)
        elif step_at == 2:
            gather_hop(hs, 4, hsend, hrecv, gsend, grecv)
    for direction, sub in near:
        last[sub] = chip_sum(0, sub) + sum_take(direction, 2, sub)
    for direction, sub in far:
        last[sub] = last[sub] + sum_take(direction, 3, sub)

    row, col = iota((4 * RBLK, 4 * CAP), 0), iota((4 * RBLK, 4 * CAP), 1)
    group = (row * 2731) >> 16
    spread = ones_where((col == row - (RBLK - CAP) * group) & (row - RBLK * group < CAP))
    for g in range(8):
        value = last[g // 4][(g % 4) * 80:(g % 4) * 80 + 80].astype(BF16)
        rout[4 * g:4 * g + 4] = mm(spread, value).astype(BF16).reshape(4, RBLK, DK)
    for o in RETURN_ORDER:
        there = lax.rem(me + o, N_EP)
        push(rout.at[lax.rem(there + x, 2) * 16 + lax.div(there, 2)], rin.at[me],
             bsend.at[o], brecv.at[o], at_ep(there))
    rin[me] = rout[lax.div(me, 2)]

    mixed += project(3) + project(5) + project(4)
    mixed_ref[...] = mixed.astype(BF16)

    for o in RETURN_ORDER:
        await_in(rin.at[lax.rem(me + N_EP - o, N_EP)], bsend.at[o], brecv.at[o])
    returned = rin[...].reshape(N_EP * RBLK, DK)
    moe_ref[...] = (mm(qh_v[...], returned) + mm(ql_v[...], returned)).astype(BF16)

    for copy in pending:
        copy.wait_send()
    for k in range(2):
        for o in SEND_ORDER:
            if o:
                dispatch(k, o).wait_send()
            else:
                @pl.when(c == 1)
                def _():
                    dispatch(k, 0).wait_send()
    for dz in range(1, NZ):
        @pl.when(z + dz < NZ)
        def _():
            along_z(dz).wait_send()


def body(
    mix_query, forget_input, mix_value, out_gate_input, decay_shift, forget_floor, head_gain,
    w_mix_out, moe_input, moe_gain, routes, route_weight, w_exp_gate, w_exp_up, w_exp_down,
):
    vmem = pl.BlockSpec(memory_space=pltpu.VMEM)
    hbm = pl.BlockSpec(memory_space=pl.ANY)
    sem = pltpu.SemaphoreType.DMA
    outs = jax.ShapeDtypeStruct((ROWS, DK), BF16)
    return pl.pallas_call(
        kernel,
        out_shape=(outs, outs),
        in_specs=[hbm] * 4 + [vmem] * 3 + [hbm] * 2 + [vmem] * 3 + [hbm] * 3,
        out_specs=(vmem, vmem),
        scratch_shapes=[
            pltpu.VMEM((4, ROWS, DK), BF16),
            pltpu.VMEM((ROWS, D), BF16),
            pltpu.VMEM((2, ROWS, FPD), BF16),
            pltpu.VMEM((D, FPD), BF16),
            pltpu.VMEM((D, FPD), BF16),
            pltpu.VMEM((NY, FPD, FPD), BF16),
            pltpu.VMEM((D, DK), BF16),
            pltpu.VMEM((2, ROWS, FPD), BF16),
            pltpu.VMEM((2, 16, DBLK, DK), BF16),
            pltpu.VMEM((2, 16, DBLK, DK), BF16),
            pltpu.VMEM((NY, 2, 2, HALF // 2, FPD), BF16),
            pltpu.VMEM((SLOTS, FPD), F32),
            pltpu.VMEM((SLOTS, FPD), F32),
            pltpu.VMEM((SLOTS, FPD), BF16),
            pltpu.VMEM((NY, SLOTS, DK), BF16),
            pltpu.VMEM((NY, SLOTS, DK), BF16),
            pltpu.VMEM((NY, SLOTS, DK), BF16),
            pltpu.VMEM((2, 4, 2, HALF, DK), BF16),
            pltpu.VMEM((2, 4, 2, HALF, DK), BF16),
            pltpu.VMEM((N_EP, RBLK, DK), BF16),
            pltpu.VMEM((N_EP, RBLK, DK), BF16),
            pltpu.VMEM((ROWS, N_EP * RBLK), BF16),
            pltpu.VMEM((ROWS, N_EP * RBLK), BF16),
            pltpu.VMEM((NX, PACK, DK), BF16),
            pltpu.VMEM((NZ, PACK, DK), BF16),
            pltpu.VMEM((2, ROWS, DK), F32),
            pltpu.VMEM((NY, 2, 2, ROWS // 2, DK), BF16),
            sem((12,)), sem((19,)), sem((32,)), sem((32,)), sem((16,)), sem((16,)),
            sem((16,)), sem((16,)), sem((8,)), sem((8,)), sem((16,)), sem((16,)),
            sem((N_EP,)), sem((N_EP,)), sem((NX,)), sem((NX,)), sem((NZ,)), sem((NZ,)),
            sem((16,)), sem((16,)), sem((16,)), sem((16,)),
        ],
        compiler_params=pltpu.CompilerParams(collective_id=0, has_side_effects=True),
        name="step",
    )(
        mix_query, forget_input, mix_value, out_gate_input,
        decay_shift.reshape(1, ROWS), forget_floor.reshape(1, DK), head_gain.reshape(1, DK),
        w_mix_out, moe_input, moe_gain.reshape(1, D), routes.T, route_weight.T,
        w_exp_gate[0], w_exp_up[0], w_exp_down[0],
    )


def solution(mesh):
    torus = Mesh(mesh.devices.reshape(NZ, NX, NY, 2), ("ep_0", "ep_1", "tp_0", "tp_1"))
    placed = (
        P(EP, TP), P(EP, TP), P(EP, TP), P(EP, TP), P(EP, TP), P(TP), P(), P(None, TP),
        P(EP, None), P(), P(EP, None), P(EP, None), P(EP, None, TP), P(EP, None, TP),
        P(EP, TP, None),
    )
    return jax.shard_map(
        body, mesh=torus, in_specs=placed, out_specs=(P(EP, TP), P(EP, TP)), check_vma=False
    )
```

time: 84.2 us -> 73.5 us (0.87); the launches traced: 84 us -> 72.4 us
  Pallas kernels: 79.9 us -> 69.6 us
  local copies, waits for them, and re-layouts: 3.43 us -> 2.14 us
    pallas_call x1, Pallas kernels: 79.9 us -> 69.6 us  [body(): pl.pallas_call(kernel, out_shape=(outs, outs), in_specs=[hbm] * 4 + [vmem...]
    unnamed x6 -> x4, local copies, waits for them, and re-layouts: 2.83 us -> 2.14 us
where the time goes in v2:
time: 73.5 us; the launch traced here: 72.4 us
  Pallas kernels  69.6 us (95%)
  local copies, waits for them, and re-layouts  2.14 us (3%)
    pallas_call x1, Pallas kernels, body(): pl.pallas_call(kernel, out_shape=(outs, outs), in_specs=[hbm] * 4 + [vmem...  69.6 us
    unnamed x4, local copies, waits for them, and re-layouts  2.14 us

profile of v2, /device:TPU:1, one launch (start us, length us, event | category | flops | bytes accessed | tf_op | source)
XLA Modules:
  0.0 72.4 jit_solution(11433923839653520710)
XLA Ops:
  0.6 69.6 %step.1 = (bf16[256,128]{1,0:T(8,128)(2,1)}, bf16[256,128]{1,0:T(8,128)(2,1)}) custom-call(bf16[256,128]{1,0:T(8,128)(2,1)} %q_hbm.1, bf16[256,128]{1,0:T(8,128)(2,1)} %f_hbm.1, bf16[256,128]{1,0:T(8,128)(2,1)} %v_hbm.1, bf16[256,128]{1,0:T(8,128)(2,1)} %og_hbm.1, f32[1,256]{1,0:T(1,128)} %bitcast.15, f32[1,128]{1,0:T(1,128)} %bitcast.16, ...), custom_call_target="tpu_custom_call" | custom-call | tf_op jit(solution)/shard_map/step/pallas_call | solution.py:544
  70.2 0.0 copy-start
  70.2 1.5 %copy.19 = bf16[256,128]{1,0:T(8,128)(2,1)} copy(bf16[256,128]{1,0:T(8,128)(2,1)} %get-tuple-element.4) | data formatting | bytes 131072
  71.7 0.0 copy-done
  71.8 0.6 copy.20
Async XLA Ops:
  70.2 1.5 %copy-start = (bf16[256,128]{1,0:T(8,128)(2,1)S(1)}, bf16[256,128]{1,0:T(8,128)(2,1)}, u32[]{:S(2)}) copy-start(bf16[256,128]{1,0:T(8,128)(2,1)} %get-tuple-element.5) | copy-start | bytes 196612

commit v3 on v2

--- a/solution.py
+++ b/solution.py
@@ -29,8 +29,8 @@
 HIGH = lax.Precision.HIGHEST
 
 SEND_ORDER = (8, 7, 9, 6, 10, 5, 11, 4, 12, 3, 13, 2, 14, 1, 15, 0)
+BACK_ORDER = (8, 9, 7, 10, 6, 11, 5, 12, 4, 13, 3, 14, 2, 15, 1, 0)
 RETURN_ORDER = sorted(range(1, N_EP), key=lambda o: -min(o, N_EP - o))
-CHUNK_ORDER = (4, 3, 5, 2, 6, 1, 7, 0)
 
 
 def ones_where(mask):
@@ -52,9 +52,10 @@
 
 
 def kernel(
-    q_hbm, f_hbm, v_hbm, og_hbm, shift_ref, floor_ref, hgain_ref, wmix_hbm,
-    moe_hbm, gain_ref, routes_ref, rw_ref, wg_hbm, wu_hbm, wd_hbm,
+    q_hbm, f_hbm, v_hbm, og_hbm, shift_hbm, floor_hbm, hgain_hbm, wmix_hbm,
+    moe_hbm, gain_hbm, routes_hbm, rw_hbm, wg_hbm, wu_hbm, wd_hbm,
     mixed_ref, moe_ref,
+    shift_ref, floor_ref, hgain_ref, gain_ref, routes_ref, rw_ref,
     mixer_v, moe_v, mine_v, wg_v, wu_v, wd_v, wmix_v, norm_v,
     sbuf, rbuf, xs, accg, accu, hid, part, pout, pin, rsend, rrecv,
     rout, rin, qh_v, ql_v, sx, sz, qd_v, hs,
@@ -91,6 +92,11 @@
     def await_in(dst, send, recv):
         remote(dst, dst, send, recv, partner).wait_recv()
 
+    first_in = [
+        pltpu.make_async_copy(routes_hbm, routes_ref, lsem.at[12]),
+        pltpu.make_async_copy(gain_hbm, gain_ref, lsem.at[13])]
+    for copy in first_in:
+        copy.start()
     rows_in = []
     for i in range(4):
         rows_in.append(pltpu.make_async_copy(
@@ -105,6 +111,11 @@
     mixer_in = [
         pltpu.make_async_copy(ref, mixer_v.at[i], lsem.at[7 + i])
         for i, ref in enumerate((f_hbm, v_hbm, q_hbm, og_hbm))]
+    mixer_in += [
+        pltpu.make_async_copy(a, b, lsem.at[14 + i])
+        for i, (a, b) in enumerate((
+            (shift_hbm, shift_ref), (floor_hbm, floor_ref), (hgain_hbm, hgain_ref),
+            (rw_hbm, rw_ref)))]
     for copy in mixer_in:
         copy.start()
 
@@ -133,6 +144,7 @@
     for copy in weights_in:
         copy.start()
 
+    first_in[0].wait()
     e0, e1 = routes_ref[0:1, :], routes_ref[1:2, :]
     ids = iota((N_EP, ROWS), 0)
     one0, one1 = ids == e0, ids == e1
@@ -148,6 +160,7 @@
         rows_in[i].wait()
     rows_in[4].wait()
     rows_in[5].wait()
+    first_in[1].wait()
     halves = (y, lax.rem(y + NY // 2, NY))
     gains = [gain_ref[:, pl.ds(pl.multiple_of(k * FPD, FPD), FPD)] for k in halves]
     for i in range(4):
@@ -194,9 +207,9 @@
                 def _():
                     own_copies[k].start()
 
-    floor = floor_ref[...]
     for copy in mixer_in:
         copy.wait()
+    floor = floor_ref[...]
     pre = mixer_v[0].astype(F32)
     forget = floor + (1.0 - floor) * jax.nn.sigmoid(pre)
     keys = (1.0 - floor) * jax.nn.sigmoid(-pre)
@@ -346,28 +359,97 @@
     weights_in[0].wait()
     weights_in[1].wait()
 
-    def expert_in(j, first=False):
-        for sub in range(2):
-            pair_take(xs, j, sub, psend, precv)
-        rows = xs[slab(j)].reshape(SLOTS, FPD)
-        depth = pl.ds(pl.multiple_of(slab(j) * FPD, FPD), FPD)
-        if first:
-            accg[...] = mm(rows, wg_v[depth, :])
-            accu[...] = mm(rows, wu_v[depth, :])
-        else:
-            accg[...] += mm(rows, wg_v[depth, :])
-            accu[...] += mm(rows, wu_v[depth, :])
+    def expert_in(half, *slabs):
+        for j in slabs:
+            pair_take(xs, j, half, psend, precv)
+            rows = jnp.concatenate([xs[slab(j), 0, half], xs[slab(j), 1, half]], axis=0)
+            depth = pl.ds(pl.multiple_of(slab(j) * FPD, FPD), FPD)
+            gate, raised = mm(rows, wg_v[depth, :]), mm(rows, wu_v[depth, :])
+            if j == 0:
+                accg[half], accu[half] = gate, raised
+            else:
+                accg[half] += gate
+                accu[half] += raised
+
+    def expert_hidden(half):
+        for i in range(2):
+            block = slice(160 * i, 160 * i + 160)
+            hid[half, block, :] = (
+                jax.nn.silu(accg[half, block, :]) * accu[half, block, :]).astype(BF16)
+
+    def expert_out(half, *slabs):
+        for j in slabs:
+            partial = mm(hid[half], wd_v[slab(j)]).astype(BF16)
+            part[j, half] = partial[:, :DK]
+            pout[j, half] = partial[:, DK:]
+            push(pout.at[j, half], pin.at[j, half],
+                 csend.at[2 * j + half], crecv.at[2 * j + half], partner)
+
+    summed = set()
+
+    def chip_sum(j, half, side):
+        if (j, half) not in summed:
+            summed.add((j, half))
+            await_in(pin.at[j, half], csend.at[2 * j + half], crecv.at[2 * j + half])
+        block = slice(160 * side, 160 * side + 160)
+        return part[j, half, block, :].astype(F32) + pin[j, half, block, :].astype(F32)
+
+    def sum_index(direction, step, side, half):
+        return (direction * 8 + step * 2 + side) * 2 + half
+
+    def sum_send(direction, step, side, half, value):
+        index = sum_index(direction, step, side, half)
+        rsend[direction, step, side, half] = value.astype(BF16)
+        push(rsend.at[direction, step, side, half], rrecv.at[direction, step, side, half],
+             ssend.at[index], srecv.at[index], up if direction == 0 else down)
+
+    def sum_take(direction, step, side, half):
+        index = sum_index(direction, step, side, half)
+        await_in(rrecv.at[direction, step, side, half], ssend.at[index], srecv.at[index])
+        return rrecv[direction, step, side, half].astype(F32)
+
+    def target(direction, side, step):
+        j = (4 if (direction, side) in far else 3) - step
+        return j % NY if direction == 0 else -j % NY
+
+    def sum_start(half, parts):
+        for direction, side in parts:
+            sum_send(direction, 0, side, half,
+                     chip_sum(target(direction, side, 0), half, side))
+
+    def sum_hop(step, half, parts):
+        for direction, side in parts:
+            value = sum_take(direction, step - 1, side, half)
+            sum_send(direction, step, side, half,
+                     value + chip_sum(target(direction, side, step), half, side))
 
     rows_hop(1, 0)
     rows_hop(1, 1)
-    expert_in(0, True)
+    expert_in(0, 0)
+    expert_in(1, 0)
     rows_hop(2, 0)
-    expert_in(1)
+    expert_in(0, 1, 7)
     rows_hop(2, 1)
-    expert_in(7)
     pack(1)
     for sub in range(2):
         pair_send(xs, 4, sub, psend, precv)
+
+    for dz in range(1, NZ):
+        @pl.when(z >= dz)
+        def _():
+            await_in(sz.at[lax.rem(z + NZ - dz, NZ)], zsend.at[dz], zrecv.at[dz])
+
+    before, _ = prefix(sz, NZ, z)
+    incoming = step(before, inside_x)[1]
+    result = qd_v[0] + nt_dot(qd_v[1], incoming, HIGH)
+    inverse = lax.rsqrt(jnp.mean(result * result, axis=1, keepdims=True) + EPS)
+    head_out = result * inverse * hgain_ref[...] * jax.nn.silu(mixer_v[3].astype(F32))
+    hs[y, c] = head_out.astype(BF16).reshape(2, ROWS // 2, DK)
+
+    gather_start(hs, hsend, hrecv, gsend, grecv)
+    expert_in(1, 1, 7)
+    for copy in weights_in[2:]:
+        copy.wait()
 
     slot0 = (e0 * RBLK + rank0).astype(F32)
     slot1 = (e1 * RBLK + rank1).astype(F32)
@@ -385,77 +467,25 @@
         ql_v[:, 256 * g:256 * g + 256] = (weight - high.astype(F32)).astype(BF16)
 
     rows_hop(3, 0)
-    expert_in(2)
-    expert_in(6)
-    expert_in(4)
-
-    for dz in range(1, NZ):
-        @pl.when(z >= dz)
-        def _():
-            await_in(sz.at[lax.rem(z + NZ - dz, NZ)], zsend.at[dz], zrecv.at[dz])
-
-    before, _ = prefix(sz, NZ, z)
-    incoming = step(before, inside_x)[1]
-    result = qd_v[0] + nt_dot(qd_v[1], incoming, HIGH)
-    inverse = lax.rsqrt(jnp.mean(result * result, axis=1, keepdims=True) + EPS)
-    head_out = result * inverse * hgain_ref[...] * jax.nn.silu(mixer_v[3].astype(F32))
-    hs[y, c] = head_out.astype(BF16).reshape(2, ROWS // 2, DK)
-
-    gather_start(hs, hsend, hrecv, gsend, grecv)
+    expert_in(0, 2, 6, 4)
+    expert_in(1, 2, 6)
+    expert_in(0, 3, 5)
+    expert_hidden(0)
+    expert_out(0, 4)
     rows_hop(3, 1)
-    expert_in(3)
-    expert_in(5)
-
-    for i in range(4):
-        block = slice(160 * i, 160 * i + 160)
-        hid[block, :] = (jax.nn.silu(accg[block, :]) * accu[block, :]).astype(BF16)
-    for copy in weights_in[3:]:
-        copy.wait()
-
-    def expert_out(j):
-        partial = mm(hid[...], wd_v[slab(j)]).astype(BF16)
-        part[j] = partial[:, :DK]
-        pout[j] = partial[:, DK:]
-        push(pout.at[j], pin.at[j], csend.at[j], crecv.at[j], partner)
-
-    def chip_sum(j, sub):
-        block = slice(HALF * sub, HALF * sub + HALF)
-        return part[j, block, :].astype(F32) + pin[j, block, :].astype(F32)
-
-    def sum_send(direction, step, sub, value):
-        index = direction * 8 + step * 2 + sub
-        rsend[direction, step, sub] = value.astype(BF16)
-        push(rsend.at[direction, step, sub], rrecv.at[direction, step, sub],
-             ssend.at[index], srecv.at[index], up if direction == 0 else down)
-
-    def sum_take(direction, step, sub):
-        index = direction * 8 + step * 2 + sub
-        await_in(rrecv.at[direction, step, sub], ssend.at[index], srecv.at[index])
-        return rrecv[direction, step, sub].astype(F32)
-
-    def ready(j):
-        await_in(pin.at[j], csend.at[j], crecv.at[j])
-
-    def target(direction, sub, step):
-        j = (4 if (direction, sub) in far else 3) - step
-        return j % NY if direction == 0 else -j % NY
-
-    for j in (4, 3, 5):
-        expert_out(j)
+    expert_out(0, 3, 5)
+    expert_in(1, 4)
+    sum_start(0, far)
+    expert_in(1, 3, 5)
+    sum_start(0, near)
+    expert_hidden(1)
+    expert_out(1, 4, 3, 5)
     gather_hop(hs, 1, hsend, hrecv, gsend, grecv)
-    ready(4)
-    for direction, sub in far:
-        sum_send(direction, 0, sub, chip_sum(target(direction, sub, 0), sub))
-    ready(3)
-    ready(5)
-    for direction, sub in near:
-        sum_send(direction, 0, sub, chip_sum(target(direction, sub, 0), sub))
-    for j in (2, 6):
-        expert_out(j)
+    expert_out(0, 2, 6)
+    sum_start(1, far)
+    sum_start(1, near)
+    expert_out(1, 2, 6)
     gather_hop(hs, 2, hsend, hrecv, gsend, grecv)
-    for j in (1, 7, 0):
-        expert_out(j)
-    weights_in[2].wait()
 
     def project(j):
         for sub in range(2):
@@ -464,56 +494,60 @@
         rows = jnp.concatenate([heads[0], heads[1]], axis=1)
         return mm(rows, wmix_v[pl.ds(pl.multiple_of(slab(j) * FPD, FPD), FPD), :])
 
-    last = {}
-    for step_at in range(1, 5):
-        if step_at == 1:
-            late = (2, 6)
-        elif step_at == 2:
-            late = (1, 7)
-        elif step_at == 3:
-            late = (0,)
-        else:
-            late = ()
-            mixed += project(1) + project(7) + project(2) + project(6)
-        for direction, sub in far:
-            if step_at < 4:
-                value = sum_take(direction, step_at - 1, sub)
-                sum_send(direction, step_at, sub,
-                         value + chip_sum(target(direction, sub, step_at), sub))
-        for j in late:
-            ready(j)
-        for direction, sub in near:
-            if step_at < 3:
-                value = sum_take(direction, step_at - 1, sub)
-                sum_send(direction, step_at, sub,
-                         value + chip_sum(target(direction, sub, step_at), sub))
-        if step_at == 1:
-            gather_hop(hs, 3, hsend, hrecv, gsend, grecv)
-            mixed = project(0)
-        elif step_at == 2:
-            gather_hop(hs, 4, hsend, hrecv, gsend, grecv)
-    for direction, sub in near:
-        last[sub] = chip_sum(0, sub) + sum_take(direction, 2, sub)
-    for direction, sub in far:
-        last[sub] = last[sub] + sum_take(direction, 3, sub)
-
     row, col = iota((4 * RBLK, 4 * CAP), 0), iota((4 * RBLK, 4 * CAP), 1)
     group = (row * 2731) >> 16
     spread = ones_where((col == row - (RBLK - CAP) * group) & (row - RBLK * group < CAP))
-    for g in range(8):
-        value = last[g // 4][(g % 4) * 80:(g % 4) * 80 + 80].astype(BF16)
-        rout[4 * g:4 * g + 4] = mm(spread, value).astype(BF16).reshape(4, RBLK, DK)
+
+    def give_back(o, half):
+        there = 16 * half + lax.rem(me + o, 16)
+        return remote(rout.at[lax.rem(there + x, 2) * 16 + lax.div(there, 2)], rin.at[me],
+                      bsend.at[16 * half + o], brecv.at[me], at_ep(there))
+
+    def finish(half):
+        for side in range(2):
+            value = chip_sum(0, half, side)
+            for direction in range(2):
+                value = value + sum_take(direction, 3 if (direction, side) in far else 2,
+                                         side, half)
+            for g in range(2):
+                place = 16 * side + 8 * half + 4 * g
+                rout[place:place + 4] = mm(
+                    spread, value[80 * g:80 * g + 80].astype(BF16)
+                ).astype(BF16).reshape(4, RBLK, DK)
+        for o in BACK_ORDER:
+            if o:
+                give_back(o, half).start()
+            else:
+                @pl.when(lax.div(me, 16) != half)
+                def _():
+                    give_back(0, half).start()
+
+    sum_hop(1, 0, far)
+    expert_out(0, 1, 7, 0)
+    sum_hop(1, 0, near)
+    sum_hop(1, 1, far)
+    expert_out(1, 1, 7, 0)
+    sum_hop(1, 1, near)
+    gather_hop(hs, 3, hsend, hrecv, gsend, grecv)
+    mixed = project(0)
+    sum_hop(2, 0, far)
+    sum_hop(2, 0, near)
+    sum_hop(2, 1, far)
+    sum_hop(2, 1, near)
+    gather_hop(hs, 4, hsend, hrecv, gsend, grecv)
+    mixed += project(1) + project(7)
+    sum_hop(3, 0, far)
+    mixed += project(2) + project(6)
+    sum_hop(3, 1, far)
+    finish(0)
+    finish(1)
+    rin[me] = rout[lax.div(me, 2)]
+    mixed += project(3) + project(5) + project(4)
+    mixed_ref[...] = mixed.astype(BF16)
+
     for o in RETURN_ORDER:
         there = lax.rem(me + o, N_EP)
-        push(rout.at[lax.rem(there + x, 2) * 16 + lax.div(there, 2)], rin.at[me],
-             bsend.at[o], brecv.at[o], at_ep(there))
-    rin[me] = rout[lax.div(me, 2)]
-
-    mixed += project(3) + project(5) + project(4)
-    mixed_ref[...] = mixed.astype(BF16)
-
-    for o in RETURN_ORDER:
-        await_in(rin.at[lax.rem(me + N_EP - o, N_EP)], bsend.at[o], brecv.at[o])
+        await_in(rin.at[there], bsend.at[o], brecv.at[there])
     returned = rin[...].reshape(N_EP * RBLK, DK)
     moe_ref[...] = (mm(qh_v[...], returned) + mm(ql_v[...], returned)).astype(BF16)
 
@@ -532,6 +566,14 @@
         def _():
             along_z(dz).wait_send()
 
+    for half in range(2):
+        for o in BACK_ORDER:
+            if o:
+                give_back(o, half).wait_send()
+            else:
+                @pl.when(lax.div(me, 16) != half)
+                def _():
+                    give_back(0, half).wait_send()
 
 def body(
     mix_query, forget_input, mix_value, out_gate_input, decay_shift, forget_floor, head_gain,
@@ -544,9 +586,15 @@
     return pl.pallas_call(
         kernel,
         out_shape=(outs, outs),
-        in_specs=[hbm] * 4 + [vmem] * 3 + [hbm] * 2 + [vmem] * 3 + [hbm] * 3,
+        in_specs=[hbm] * 15,
         out_specs=(vmem, vmem),
         scratch_shapes=[
+            pltpu.VMEM((1, ROWS), F32),
+            pltpu.VMEM((1, DK), F32),
+            pltpu.VMEM((1, DK), F32),
+            pltpu.VMEM((1, D), F32),
+            pltpu.VMEM((2, ROWS), I32),
+            pltpu.VMEM((2, ROWS), F32),
             pltpu.VMEM((4, ROWS, DK), BF16),
             pltpu.VMEM((ROWS, D), BF16),
             pltpu.VMEM((2, ROWS, FPD), BF16),
@@ -558,14 +606,14 @@
             pltpu.VMEM((2, 16, DBLK, DK), BF16),
             pltpu.VMEM((2, 16, DBLK, DK), BF16),
             pltpu.VMEM((NY, 2, 2, HALF // 2, FPD), BF16),
-            pltpu.VMEM((SLOTS, FPD), F32),
-            pltpu.VMEM((SLOTS, FPD), F32),
-            pltpu.VMEM((SLOTS, FPD), BF16),
-            pltpu.VMEM((NY, SLOTS, DK), BF16),
-            pltpu.VMEM((NY, SLOTS, DK), BF16),
-            pltpu.VMEM((NY, SLOTS, DK), BF16),
-            pltpu.VMEM((2, 4, 2, HALF, DK), BF16),
-            pltpu.VMEM((2, 4, 2, HALF, DK), BF16),
+            pltpu.VMEM((2, HALF, FPD), F32),
+            pltpu.VMEM((2, HALF, FPD), F32),
+            pltpu.VMEM((2, HALF, FPD), BF16),
+            pltpu.VMEM((NY, 2, HALF, DK), BF16),
+            pltpu.VMEM((NY, 2, HALF, DK), BF16),
+            pltpu.VMEM((NY, 2, HALF, DK), BF16),
+            pltpu.VMEM((2, 4, 2, 2, HALF // 2, DK), BF16),
+            pltpu.VMEM((2, 4, 2, 2, HALF // 2, DK), BF16),
             pltpu.VMEM((N_EP, RBLK, DK), BF16),
             pltpu.VMEM((N_EP, RBLK, DK), BF16),
             pltpu.VMEM((ROWS, N_EP * RBLK), BF16),
@@ -574,8 +622,8 @@
             pltpu.VMEM((NZ, PACK, DK), BF16),
             pltpu.VMEM((2, ROWS, DK), F32),
             pltpu.VMEM((NY, 2, 2, ROWS // 2, DK), BF16),
-            sem((12,)), sem((19,)), sem((32,)), sem((32,)), sem((16,)), sem((16,)),
-            sem((16,)), sem((16,)), sem((8,)), sem((8,)), sem((16,)), sem((16,)),
+            sem((18,)), sem((19,)), sem((32,)), sem((32,)), sem((16,)), sem((16,)),
+            sem((16,)), sem((16,)), sem((16,)), sem((16,)), sem((32,)), sem((32,)),
             sem((N_EP,)), sem((N_EP,)), sem((NX,)), sem((NX,)), sem((NZ,)), sem((NZ,)),
             sem((16,)), sem((16,)), sem((16,)), sem((16,)),
         ],

time: 73.5 us -> 72.5 us (0.986); the launches traced: 72.4 us -> 72.3 us
  no operation moved by 1% of the time
where the time goes in v3:
time: 72.5 us; the launch traced here: 72.3 us
  Pallas kernels  69.5 us (96%)
  local copies, waits for them, and re-layouts  2.14 us (3%)
    pallas_call x1, Pallas kernels, body(): pl.pallas_call(kernel, out_shape=(outs, outs), in_specs=[hbm] * 15, out_s...  69.5 us
    unnamed x4, local copies, waits for them, and re-layouts  2.14 us

profile of v3, /device:TPU:1, one launch (start us, length us, event | category | flops | bytes accessed | tf_op | source)
XLA Modules:
  0.0 72.3 jit_solution(8184118937613520024)
XLA Ops:
  0.6 69.5 %step.1 = (bf16[256,128]{1,0:T(8,128)(2,1)}, bf16[256,128]{1,0:T(8,128)(2,1)}) custom-call(bf16[256,128]{1,0:T(8,128)(2,1)} %q_hbm.1, bf16[256,128]{1,0:T(8,128)(2,1)} %f_hbm.1, bf16[256,128]{1,0:T(8,128)(2,1)} %v_hbm.1, bf16[256,128]{1,0:T(8,128)(2,1)} %og_hbm.1, f32[1,256]{1,0:T(1,128)} %bitcast.15, f32[1,128]{1,0:T(1,128)} %bitcast.16, ...), custom_call_target="tpu_custom_call" | custom-call | tf_op jit(solution)/shard_map/step/pallas_call | solution.py:586
  70.2 0.0 copy-start
  70.2 1.5 %copy.19 = bf16[256,128]{1,0:T(8,128)(2,1)} copy(bf16[256,128]{1,0:T(8,128)(2,1)} %get-tuple-element.4) | data formatting | bytes 131072
  71.7 0.0 copy-done
  71.7 0.6 copy.20
Async XLA Ops:
  70.2 1.5 %copy-start = (bf16[256,128]{1,0:T(8,128)(2,1)S(1)}, bf16[256,128]{1,0:T(8,128)(2,1)}, u32[]{:S(2)}) copy-start(bf16[256,128]{1,0:T(8,128)(2,1)} %get-tuple-element.5) | copy-start | bytes 196612

commit v4 on v3

--- a/solution.py
+++ b/solution.py
@@ -485,7 +485,6 @@
     sum_start(1, far)
     sum_start(1, near)
     expert_out(1, 2, 6)
-    gather_hop(hs, 2, hsend, hrecv, gsend, grecv)
 
     def project(j):
         for sub in range(2):
@@ -528,19 +527,19 @@
     sum_hop(1, 1, far)
     expert_out(1, 1, 7, 0)
     sum_hop(1, 1, near)
-    gather_hop(hs, 3, hsend, hrecv, gsend, grecv)
     mixed = project(0)
-    sum_hop(2, 0, far)
-    sum_hop(2, 0, near)
-    sum_hop(2, 1, far)
-    sum_hop(2, 1, near)
-    gather_hop(hs, 4, hsend, hrecv, gsend, grecv)
+    for half in range(2):
+        sum_hop(2, half, far)
+        sum_hop(2, half, near)
     mixed += project(1) + project(7)
     sum_hop(3, 0, far)
-    mixed += project(2) + project(6)
     sum_hop(3, 1, far)
+    gather_hop(hs, 2, hsend, hrecv, gsend, grecv)
     finish(0)
     finish(1)
+    gather_hop(hs, 3, hsend, hrecv, gsend, grecv)
+    mixed += project(2) + project(6)
+    gather_hop(hs, 4, hsend, hrecv, gsend, grecv)
     rin[me] = rout[lax.div(me, 2)]
     mixed += project(3) + project(5) + project(4)
     mixed_ref[...] = mixed.astype(BF16)
@@ -575,6 +574,11 @@
                 def _():
                     give_back(0, half).wait_send()
 
+def settle(a_ref, b_ref, mixed_ref, moe_ref):
+    mixed_ref[...] = a_ref[...]
+    moe_ref[...] = b_ref[...]
+
+
 def body(
     mix_query, forget_input, mix_value, out_gate_input, decay_shift, forget_floor, head_gain,
     w_mix_out, moe_input, moe_gain, routes, route_weight, w_exp_gate, w_exp_up, w_exp_down,
@@ -583,7 +587,7 @@
     hbm = pl.BlockSpec(memory_space=pl.ANY)
     sem = pltpu.SemaphoreType.DMA
     outs = jax.ShapeDtypeStruct((ROWS, DK), BF16)
-    return pl.pallas_call(
+    parts = pl.pallas_call(
         kernel,
         out_shape=(outs, outs),
         in_specs=[hbm] * 15,
@@ -635,6 +639,13 @@
         w_mix_out, moe_input, moe_gain.reshape(1, D), routes.T, route_weight.T,
         w_exp_gate[0], w_exp_up[0], w_exp_down[0],
     )
+    return pl.pallas_call(
+        settle,
+        out_shape=(outs, outs),
+        in_specs=[vmem] * 2,
+        out_specs=(vmem, vmem),
+        name="settle",
+    )(*parts)
 
 
 def solution(mesh):

time: 72.5 us -> 69.8 us (0.963)
  local copies, waits for them, and re-layouts: 2.14 us -> 0 us
    unnamed x4 -> x0, local copies, waits for them, and re-layouts: 2.14 us -> none
    pallas_call x1, Pallas kernels: 69.5 us -> 67.5 us  [body(): pl.pallas_call(kernel, out_shape=(outs, outs), in_specs=[hbm] * 15, out_s...]
    pallas_call x0 -> x1, Pallas kernels: none -> 1.53 us  [body(): pl.pallas_call(settle, out_shape=(outs, outs), in_specs=[vmem] * 2, out_s...]
where the time goes in v4:
time: 69.8 us; the launch traced here: 69.6 us
  Pallas kernels  69 us (99%)
    pallas_call x1, Pallas kernels, body(): pl.pallas_call(kernel, out_shape=(outs, outs), in_specs=[hbm] * 15, out_s...  67.5 us
    pallas_call x1, Pallas kernels, body(): pl.pallas_call(settle, out_shape=(outs, outs), in_specs=[vmem] * 2, out_s...  1.53 us

profile of v4, /device:TPU:1, one launch (start us, length us, event | category | flops | bytes accessed | tf_op | source)
XLA Modules:
  0.0 69.6 jit_solution(6924906662222747500)
XLA Ops:
  0.6 67.5 %step.1 = (bf16[256,128]{1,0:T(8,128)(2,1)}, bf16[256,128]{1,0:T(8,128)(2,1)}) custom-call(bf16[256,128]{1,0:T(8,128)(2,1)} %q_hbm.1, bf16[256,128]{1,0:T(8,128)(2,1)} %f_hbm.1, bf16[256,128]{1,0:T(8,128)(2,1)} %v_hbm.1, bf16[256,128]{1,0:T(8,128)(2,1)} %og_hbm.1, f32[1,256]{1,0:T(1,128)} %bitcast.15, f32[1,128]{1,0:T(1,128)} %bitcast.16, ...), custom_call_target="tpu_custom_call" | custom-call | tf_op jit(solution)/shard_map/step/pallas_call | solution.py:590
  68.1 1.5 %settle.1 = (bf16[256,128]{1,0:T(8,128)(2,1)}, bf16[256,128]{1,0:T(8,128)(2,1)}) custom-call(bf16[256,128]{1,0:T(8,128)(2,1)} %get-tuple-element.4.a_ref, bf16[256,128]{1,0:T(8,128)(2,1)} %get-tuple-element.5.b_ref), custom_call_target="tpu_custom_call" | custom-call | tf_op jit(solution)/shard_map/settle/pallas_call | solution.py:642

commit v5 on v4

--- a/solution.py
+++ b/solution.py
@@ -68,6 +68,10 @@
     y = lax.axis_index("tp_0")
     c = lax.axis_index("tp_1")
     me = z * NX + x
+
+    def place_of(e):
+        row = lax.div(e, NX)
+        return lax.rem(row, 2) * 8 + lax.div(row, 2) * 2 + lax.rem(lax.div(e, 2), 2)
 
     def at_ep(e):
         return (lax.div(e, NX), lax.rem(e, NX), y, c)
@@ -156,45 +160,46 @@
     rank1 = jnp.sum(
         jnp.where(one1, earlier[N_EP:] + total0, 0.0), axis=0, keepdims=True).astype(I32)
 
-    for i in range(4):
-        rows_in[i].wait()
-    rows_in[4].wait()
-    rows_in[5].wait()
-    first_in[1].wait()
-    halves = (y, lax.rem(y + NY // 2, NY))
-    gains = [gain_ref[:, pl.ds(pl.multiple_of(k * FPD, FPD), FPD)] for k in halves]
-    for i in range(4):
-        block = moe_v[64 * i:64 * i + 64, :].astype(F32)
-        mean = jnp.sum(block * block, axis=1, keepdims=True) * (1.0 / D)
-        for k in range(2):
-            own = mine_v[k, 64 * i:64 * i + 64, :].astype(F32)
-            norm_v[k, 64 * i:64 * i + 64, :] = (
-                own * lax.rsqrt(mean + EPS) * gains[k]).astype(BF16)
-
     parity = lax.rem(x + c, 2)
     target0 = jnp.where((e0 & 1) == parity, (e0 >> 1) * DBLK + rank0, -1000)
     target1 = jnp.where((e1 & 1) == parity, (e1 >> 1) * DBLK + rank1, -1000)
-    n0 = jnp.concatenate([norm_v[0, :, :DK], norm_v[1, :, :DK]], axis=1)
-    n1 = jnp.concatenate([norm_v[0, :, DK:], norm_v[1, :, DK:]], axis=1)
-    for g in range(4):
-        spot = iota((4 * DBLK, ROWS), 0) + 4 * DBLK * g
-        first = ones_where((spot == target0) | (spot == target1))
-        second = ones_where((spot == target0 + CAP) | (spot == target1 + CAP))
-        rows = (mm(first, n0) + mm(second, n1)).astype(BF16)
-        for k in range(2):
-            sbuf[k, 4 * g:4 * g + 4] = rows[:, k * DK:(k + 1) * DK].reshape(4, DBLK, DK)
-
+    halves = (y, lax.rem(y + NY // 2, NY))
+    first_in[1].wait()
+    inverses = []
+    for i in range(4):
+        rows_in[i].wait()
+        block = moe_v[64 * i:64 * i + 64, :].astype(F32)
+        mean = jnp.sum(block * block, axis=1, keepdims=True) * (1.0 / D)
+        inverses.append(lax.rsqrt(mean + EPS))
+
+    def fill(k):
+        rows_in[4 + k].wait()
+        gain = gain_ref[:, pl.ds(pl.multiple_of(halves[k] * FPD, FPD), FPD)]
+        for i in range(4):
+            own = mine_v[k, 64 * i:64 * i + 64, :].astype(F32)
+            norm_v[k, 64 * i:64 * i + 64, :] = (own * inverses[i] * gain).astype(BF16)
+        n0, n1 = norm_v[k, :, :DK], norm_v[k, :, DK:]
+        for g in range(4):
+            spot = iota((4 * DBLK, ROWS), 0) + 4 * DBLK * g
+            first = ones_where((spot == target0) | (spot == target1))
+            second = ones_where((spot == target0 + CAP) | (spot == target1 + CAP))
+            rows = (mm(first, n0) + mm(second, n1)).astype(BF16)
+            sbuf[k, 4 * g:4 * g + 4] = rows.reshape(4, DBLK, DK)
+
+    fill(0)
     pl.semaphore_wait(barrier, N_EP + 2)
 
     def dispatch(k, o):
         expert = lax.rem(me + 2 * o + c, N_EP)
-        return remote(sbuf.at[k, lax.div(expert, 2)], rbuf.at[k, lax.div(me, 2)],
+        return remote(sbuf.at[k, lax.div(expert, 2)], rbuf.at[k, place_of(me)],
                       dsend.at[16 * k + o], drecv.at[16 * k + o], at_ep(expert))
 
     own_copies = [pltpu.make_async_copy(
-        sbuf.at[k, lax.div(me, 2)], rbuf.at[k, lax.div(me, 2)], lsem.at[k * 6 + 5])
+        sbuf.at[k, lax.div(me, 2)], rbuf.at[k, place_of(me)], lsem.at[k * 6 + 5])
         for k in range(2)]
     for k in range(2):
+        if k:
+            fill(k)
         for o in SEND_ORDER:
             if o:
                 dispatch(k, o).start()
@@ -231,7 +236,7 @@
     def arrived(k):
         for o in SEND_ORDER:
             source = lax.rem(me + N_EP - 2 * o + N_EP - c, N_EP)
-            slot = rbuf.at[k, lax.div(source, 2)]
+            slot = rbuf.at[k, place_of(source)]
             if o:
                 await_in(slot, dsend.at[16 * k + o], drecv.at[16 * k + o])
             else:
@@ -498,8 +503,9 @@
     spread = ones_where((col == row - (RBLK - CAP) * group) & (row - RBLK * group < CAP))
 
     def give_back(o, half):
-        there = 16 * half + lax.rem(me + o, 16)
-        return remote(rout.at[lax.rem(there + x, 2) * 16 + lax.div(there, 2)], rin.at[me],
+        spot = lax.rem(lax.div(z, 2) * NX + x + o, 16)
+        there = (lax.div(spot, NX) * 2 + half) * NX + lax.rem(spot, NX)
+        return remote(rout.at[lax.rem(there + x, 2) * 16 + place_of(there)], rin.at[me],
                       bsend.at[16 * half + o], brecv.at[me], at_ep(there))
 
     def finish(half):
@@ -517,7 +523,7 @@
             if o:
                 give_back(o, half).start()
             else:
-                @pl.when(lax.div(me, 16) != half)
+                @pl.when(lax.rem(z, 2) != half)
                 def _():
                     give_back(0, half).start()
 
@@ -540,7 +546,7 @@
     gather_hop(hs, 3, hsend, hrecv, gsend, grecv)
     mixed += project(2) + project(6)
     gather_hop(hs, 4, hsend, hrecv, gsend, grecv)
-    rin[me] = rout[lax.div(me, 2)]
+    rin[me] = rout[place_of(me)]
     mixed += project(3) + project(5) + project(4)
     mixed_ref[...] = mixed.astype(BF16)
 
@@ -570,7 +576,7 @@
             if o:
                 give_back(o, half).wait_send()
             else:
-                @pl.when(lax.div(me, 16) != half)
+                @pl.when(lax.rem(z, 2) != half)
                 def _():
                     give_back(0, half).wait_send()
 

time: 69.8 us -> 69.3 us (level)
  no operation moved by 1% of the time
where the time goes in v5:
time: 69.3 us; the launch traced here: 69.1 us
  Pallas kernels  68.5 us (99%)
    pallas_call x1, Pallas kernels, body(): pl.pallas_call(kernel, out_shape=(outs, outs), in_specs=[hbm] * 15, out_s...  67 us
    pallas_call x1, Pallas kernels, body(): pl.pallas_call(settle, out_shape=(outs, outs), in_specs=[vmem] * 2, out_s...  1.53 us

profile of v5, /device:TPU:1, one launch (start us, length us, event | category | flops | bytes accessed | tf_op | source)
XLA Modules:
  0.0 69.1 jit_solution(2512995394583523403)
XLA Ops:
  0.6 67.0 %step.1 = (bf16[256,128]{1,0:T(8,128)(2,1)}, bf16[256,128]{1,0:T(8,128)(2,1)}) custom-call(bf16[256,128]{1,0:T(8,128)(2,1)} %q_hbm.1, bf16[256,128]{1,0:T(8,128)(2,1)} %f_hbm.1, bf16[256,128]{1,0:T(8,128)(2,1)} %v_hbm.1, bf16[256,128]{1,0:T(8,128)(2,1)} %og_hbm.1, f32[1,256]{1,0:T(1,128)} %bitcast.15, f32[1,128]{1,0:T(1,128)} %bitcast.16, ...), custom_call_target="tpu_custom_call" | custom-call | tf_op jit(solution)/shard_map/step/pallas_call | solution.py:596
  67.6 1.5 %settle.1 = (bf16[256,128]{1,0:T(8,128)(2,1)}, bf16[256,128]{1,0:T(8,128)(2,1)}) custom-call(bf16[256,128]{1,0:T(8,128)(2,1)} %get-tuple-element.4.a_ref, bf16[256,128]{1,0:T(8,128)(2,1)} %get-tuple-element.5.b_ref), custom_call_target="tpu_custom_call" | custom-call | tf_op jit(solution)/shard_map/settle/pallas_call | solution.py:648
